TPU v7x, 512 devices: a whole 4x8x8 slice. The times are simulated.
512 devices in a mesh: sp: 64 (over z, y), tp: 8 (over x, core).
Axes of the slice: x: 4, y: 8, z: 8, core: 2. Of those that a mesh axis runs over, the one named last changes fastest.
Arguments:
- tokens: bfloat16 [16384, 2048], P('sp', 'tp'), may hold values from -6 to 6
- norm_gain: float32 [2048], replicated, may hold values from 0.1 to 1.9
- recur_query: bfloat16 [2048, 1024], P(None, 'tp'), may hold values from -0.125 to 0.125
- recur_forget: bfloat16 [2048, 1024], P(None, 'tp'), may hold values from -0.125 to 0.125
- recur_value: bfloat16 [2048, 1024], P(None, 'tp'), may hold values from -0.125 to 0.125
- gate_floor: float32 [1024], P('tp'), may hold values from 0.5 to 1
- extra_decay: float32 [16384, 8], P('sp', 'tp'), may hold values from 0 to 2
- start_state: float32 [8, 128, 128], P('tp'), may hold values from -0.0625 to 0.0625
- recur_gain: float32 [1024], P('tp'), may hold values from 0.1 to 1.9
- attend_query: bfloat16 [2048, 1024], P(None, 'tp')
- attend_key: bfloat16 [2048, 1024], P(None, 'tp')
- attend_value: bfloat16 [2048, 1024], P(None, 'tp'), may hold values from -0.125 to 0.125
- gate_cache: float32 [16384, 16], P(None, 'tp'), may hold values from -16384 to 0, as said below
- attend_gain: float32 [1024], P('tp'), may hold values from 0.1 to 1.9
- recur_output: bfloat16 [1024, 2048], P(None, 'tp'), may hold values from -0.1875 to 0.1875
- attend_output: bfloat16 [1024, 2048], P(None, 'tp'), may hold values from -0.1875 to 0.1875
Outputs:
- layer_output: bfloat16 [16384, 2048], P('sp', 'tp')
Inputs may be any that keep to these rules, and one draw needn't show every extreme that they name: `gate_cache`: never rising along positions.
All inputs are finite; a program needn't handle non-finite values.
Results may differ from a plain program's by a relative error of at most 0.018.
Values may be sent and summed in bfloat16 or wider, within the bound.
A program may use at most 64 MiB of HBM per device.

v0:
```python
import jax
import jax.numpy as jnp
from jax import lax
from jax.sharding import Mesh
from jax.sharding import PartitionSpec as P

FD = 64
SP = ("sp_0", "sp_1")


EPSILON = 1e-06
TOP_PRECISION = lax.Precision.HIGHEST


def copy_for_each(x, axis):
    devices = lax.axis_size(axis)
    return lax.all_to_all(jnp.broadcast_to(x[None], (devices, *x.shape)), axis, 0, 0, tiled=True)


def laid_out(pieces, dim):
    shape = list(pieces.shape[1:])
    shape[dim] *= pieces.shape[0]
    return jnp.moveaxis(pieces, 0, dim).reshape(shape)


def gather_directly(x, axis, dim):
    pieces = copy_for_each(x, axis)
    return laid_out(pieces, dim)


def neutral_like(x, identity):
    return jax.tree.map(
        lambda part, zero: jnp.zeros_like(part) + jnp.asarray(zero, part.dtype), x, identity
    )


def collected_together(x, axis):
    leaves = jax.tree.leaves(x)
    sequence = sorted(range(len(leaves)), key=lambda k: -leaves[k].size)
    width = (1, *leaves[sequence[0]].shape)[-1]
    lines = [
        jnp.pad(leaves[k].reshape(-1), (0, -leaves[k].size % width)).reshape(-1, width)
        for k in sequence
    ]
    both, at, found = (lax.all_gather(jnp.concatenate(lines), axis), 0, {})
    for k, line in zip(sequence, lines):
        piece = both[:, at : at + len(line)].reshape(len(both), -1)
        found[k] = piece[:, : leaves[k].size].reshape(-1, *leaves[k].shape)
        at += len(line)
    numbers = iter(range(len(leaves)))
    return jax.tree.map(lambda _: found[next(numbers)], x)


def entering(x, axes, combine, identity):
    before = start = neutral_like(x, identity)
    subtotal = x
    for axis in reversed(axes):
        devices, position = (lax.axis_size(axis), lax.axis_index(axis))
        pieces = collected_together(
            jax.tree.map(
                lambda part, kind: part.astype(kind), subtotal, (jnp.bfloat16, jnp.bfloat16)
            ),
            axis,
        )
        inside, subtotal = (start, start)
        for k in range(devices):
            passed = k < position
            subtotal = combine(
                subtotal, jax.tree.map(lambda part, own: part[k].astype(own.dtype), pieces, x)
            )
            inside = jax.tree.map(lambda new, old: jnp.where(passed, new, old), subtotal, inside)
        before = combine(inside, before)
    return before


def side_by_side(arrays, axis, dim, along):
    widths = [a.shape[along] for a in arrays]
    both = jnp.concatenate(arrays, axis=along)
    out = lax.all_gather(both, axis, axis=dim, tiled=True)
    return tuple(jnp.split(out, [sum(widths[:k]) for k in range(1, len(widths))], axis=along))


def head_norm(per_head, head_gain):
    normed = per_head * lax.rsqrt(jnp.mean(per_head * per_head, axis=-1, keepdims=True) + EPSILON)
    return normed.reshape(per_head.shape[0], -1) * head_gain


def local_recurrence(query_rows, decays, inflow, values):
    span_len = min(64, query_rows.shape[0])
    blocks = query_rows.shape[0] // span_len

    def to_blocks(tensor):
        return tensor.reshape(blocks, span_len, tensor.shape[1], tensor.shape[2])

    causal = jnp.tril(jnp.ones((span_len, span_len), dtype=bool))[:, :, None, None]

    def advance(carried_state, pieces):
        query_block, g_block, k_block, value_block = pieces
        running_total = jnp.cumsum(g_block, axis=0)
        offsets = jnp.where(causal, running_total[:, None] - running_total[None, :], -jnp.inf)
        mixing = jnp.einsum(
            "thk,shk,tshk->hts", query_block, k_block, jnp.exp(offsets), precision=TOP_PRECISION
        )
        final_result = jnp.einsum("hts,shv->thv", mixing, value_block, precision=TOP_PRECISION)
        final_result = final_result + jnp.einsum(
            "dzc,zcu->dzu",
            query_block * jnp.exp(running_total),
            carried_state,
            precision=TOP_PRECISION,
        )
        ending_state = running_total[-1]
        weighted_values = k_block * jnp.exp(ending_state[None] - running_total)
        carried_state = jnp.exp(ending_state)[..., None] * carried_state + jnp.einsum(
            "cun,cub->unb", weighted_values, value_block, precision=TOP_PRECISION
        )
        return (carried_state, final_result)

    initial = jnp.zeros((query_rows.shape[1], query_rows.shape[2], values.shape[2]), jnp.float32)
    final_state, results = lax.scan(
        advance,
        initial,
        (to_blocks(query_rows), to_blocks(decays), to_blocks(inflow), to_blocks(values)),
    )
    return (results.reshape(query_rows.shape[0], query_rows.shape[1], values.shape[2]), final_state)


def row_projector(weight, carried_state, section):
    return carried_state + jnp.dot(section, weight, preferred_element_type=jnp.float32)


def keep_state(running_state):
    return running_state


def block_update(
    group_query, group_gates, group_index, key_rows, value_rows, key_gates, key_index, scaling
):

    def compute(running_state):
        maxima, totals, summed = running_state
        scores = (
            jnp.einsum("qhd,khd->hqk", group_query, key_rows, preferred_element_type=jnp.float32)
            * scaling
        )
        scores = scores + group_gates.T[:, :, None] - key_gates.T[:, None, :]
        allowed = (key_index[None, :] <= group_index[:, None])[None]
        highest = jnp.maximum(maxima, jnp.max(jnp.where(allowed, scores, -1e30), axis=-1))
        weights = jnp.where(allowed, jnp.exp(scores - highest[..., None]), 0.0)
        rescale = jnp.exp(maxima - highest)
        totals = totals * rescale + jnp.sum(weights, axis=-1)
        summed = summed * rescale.T[:, :, None] + jnp.einsum(
            "hqk,khd->qhd",
            weights.astype(jnp.bfloat16),
            value_rows,
            preferred_element_type=jnp.float32,
        )
        return (highest, totals, summed)

    return compute


def shards(
    tokens,
    norm_gain,
    recur_query,
    recur_forget,
    recur_value,
    gate_floor,
    extra_decay,
    start_state,
    recur_gain,
    attend_query,
    attend_key,
    attend_value,
    gate_cache,
    attend_gain,
    recur_output,
    attend_output,
):
    height = tokens.shape[0]
    model_width = norm_gain.shape[0]
    inputs = (recur_query, recur_forget, recur_value, attend_query, attend_key, attend_value)
    wide = gather_directly(tokens, "tp", 1).astype(jnp.float32)
    scaled = (wide * norm_gain).astype(jnp.bfloat16)
    updated = tuple(
        (jnp.dot(scaled, weight, preferred_element_type=jnp.float32) for weight in inputs)
    )
    products = updated
    squares = jnp.sum(wide * wide, axis=1, keepdims=True)
    inverse = lax.rsqrt(squares / model_width + EPSILON)
    projected = tuple(
        ((partial_value * inverse).astype(jnp.bfloat16) for partial_value in products)
    )
    rec_heads = start_state.shape[0]
    query_rows = projected[0].astype(jnp.float32).reshape(height, rec_heads, -1)
    forget_pre = projected[1].astype(jnp.float32).reshape(height, rec_heads, -1)
    values = projected[2].astype(jnp.float32).reshape(height, rec_heads, -1)
    inflow = (1.0 - gate_floor.reshape(rec_heads, -1)) * jax.nn.sigmoid(-forget_pre)
    decays = jnp.log1p(-inflow) - extra_decay[:, :, None]
    local_out, final_state = local_recurrence(query_rows, decays, inflow, values)
    running_total = jnp.cumsum(decays, axis=0)
    overall = running_total[-1]

    def compose(earlier, latter):
        return (earlier[0] * latter[0], latter[0][..., None] * earlier[1] + latter[1])

    identity = (jnp.ones_like(overall), jnp.zeros_like(final_state))
    passed, arriving = entering((jnp.exp(overall), final_state), SP, compose, identity)
    incoming_rows = passed[..., None] * start_state + arriving
    carried_out = jnp.einsum(
        "dzc,zcu->dzu", query_rows * jnp.exp(running_total), incoming_rows, precision=TOP_PRECISION
    )
    rec_rows = head_norm(local_out + carried_out, recur_gain).astype(jnp.bfloat16)
    out_width = recur_output.shape[1]
    layer_sum = row_projector(
        recur_output,
        jnp.zeros((height, out_width), jnp.float32),
        gather_directly(rec_rows, "tp", 1),
    )
    att_heads = gate_cache.shape[1]
    att_query = projected[3].reshape(height, att_heads, FD)
    offset = lax.axis_index(SP) * height
    scaling = FD ** (-0.5)
    groups = ((att_query, offset, height),)
    prepared = tuple(
        (
            (
                group_query,
                lax.dynamic_slice_in_dim(gate_cache, group_start, rows, 0),
                group_start + jnp.arange(rows),
            )
            for group_query, group_start, rows in groups
        )
    )
    initial = tuple(
        (
            (
                jnp.full((att_heads, rows), -1e30, jnp.float32),
                jnp.zeros((att_heads, rows), jnp.float32),
                jnp.zeros((rows, att_heads, FD), jnp.float32),
            )
            for _, _, rows in groups
        )
    )
    key_part, value_part = side_by_side((projected[4], projected[5]), SP, 0, 1)
    total_amount = key_part.shape[0]
    step_rows = 2 * height

    def advance_keys(number, states):
        begin_at = number * step_rows
        key_rows = lax.dynamic_slice_in_dim(key_part, begin_at, step_rows, 0).reshape(
            step_rows, att_heads, FD
        )
        value_rows = lax.dynamic_slice_in_dim(value_part, begin_at, step_rows, 0).reshape(
            step_rows, att_heads, FD
        )
        key_gates = lax.dynamic_slice_in_dim(gate_cache, begin_at, step_rows, 0)
        key_index = begin_at + jnp.arange(step_rows)
        updated = []
        for (group_query, group_gates, group_index), state in zip(prepared, states):
            compute = block_update(
                group_query,
                group_gates,
                group_index,
                key_rows,
                value_rows,
                key_gates,
                key_index,
                scaling,
            )
            needed = begin_at <= group_index[-1]
            updated.append(lax.cond(needed, compute, keep_state, state))
        return tuple(updated)

    folded = lax.fori_loop(0, total_amount // step_rows, advance_keys, initial)
    row_parts = [
        head_norm(summed / totals.T[:, :, None], attend_gain).astype(jnp.bfloat16)
        for maxima, totals, summed in folded
    ]
    att_rows = row_parts[0]
    layer_sum = row_projector(attend_output, layer_sum, gather_directly(att_rows, "tp", 1))
    return layer_sum.astype(jnp.bfloat16)


def solution(mesh):
    finer = Mesh(mesh.devices.reshape(8, 8, mesh.shape["tp"]), ("sp_0", "sp_1", "tp"))
    return jax.shard_map(
        shards,
        mesh=finer,
        in_specs=(
            P(SP, "tp"),
            P(),
            P(None, "tp"),
            P(None, "tp"),
            P(None, "tp"),
            P("tp"),
            P(SP, "tp"),
            P("tp", None, None),
            P("tp"),
            P(None, "tp"),
            P(None, "tp"),
            P(None, "tp"),
            P(None, "tp"),
            P("tp"),
            P(None, "tp"),
            P(None, "tp"),
        ),
        out_specs=P(SP, "tp"),
        check_vma=False,
    )
```

profile of v0, /device:TPU:496, one launch (start us, length us, event | category | flops | bytes accessed | tf_op | source)
XLA Modules:
  0.0 304.5 jit_solution(15076468607059379634)
XLA Ops:
  7.7 20.1 %all_to_all.15 = bf16[8,256,256]{1,2,0:T(8,128)(2,1)S(1)} all-to-all(bf16[8,256,256]{1,2,0:T(8,128)(2,1)S(1)} %broadcast_in_dim.62), channel_id=1, replica_groups=mesh['sp_0'=8,'sp_1'=8,'tp'=8] {'tp'}, dimensions={0} | all-to-all | bytes 2097152 | tf_op jit(solution)/shard_map/all_to_all | solution.py:17
  33.6 13.0 %while.31 = (s32[]{:T(128)}, f32[1,128,128]{2,1,0:T(8,128)S(1)}, f32[4,64,1,128]{3,1,2,0:T(8,128)S(1)}, f32[4,64,1,128]{3,1,2,0:T(8,128)S(1)}, f32[4,64,1,128]{3...) while((s32[]{:T(128)}, f32[1,128,128]{2,1,0:T(8,128)S(1)}, ...), condition=%wide.region_3.4_spmd.clone, body=%wide.region_1.3_spmd.clone.sunk | while | flops 34693120 | bytes 5156984 | solution.py:119
  46.9 24.5 %all-gather.2 = bf16[8,129,128]{2,1,0:T(8,128)(2,1)S(1)} all-gather(bf16[1,129,128]{2,1,0:T(8,128)(2,1)S(1)} %maximum_bitcast_fusion), channel_id=2, replica_groups=mesh['sp_0'=8,'sp_1'=8,'tp'=8] {'sp_1'}, dimensions={0}, use_global_device_ids=true | all-gather | bytes 297216 | tf_op jit(solution)/shard_map/all_gather | solution.py:45
  71.6 25.6 %all-gather.3 = bf16[8,129,128]{2,1,0:T(8,128)(2,1)S(1)} all-gather(bf16[1,129,128]{2,1,0:T(8,128)(2,1)S(1)} %maximum_bitcast_fusion.1), channel_id=3, replica_groups=mesh['sp_0'=8,'sp_1'=8,'tp'=8] {'sp_0'}, dimensions={0}, use_global_device_ids=true | all-gather | bytes 297216 | tf_op jit(solution)/shard_map/all_gather | solution.py:45
  99.0 3.5 %all-to-all-start.1 = ((bf16[8,256,128]{1,2,0:T(8,128)(2,1)}), bf16[8,256,128]{1,2,0:T(8,128)(2,1)S(1)}, u32[]{:S(2)}, u32[]{:S(2)}) async-start(bf16[8,256,128]{1,2,0:T(8,128)(2,1)} %broadcast_in_dim.63), calls=%async_computation.1 | async-start | bytes 1048576 | tf_op jit(solution)/shard_map/all_to_all | solution.py:17
  102.5 22.9 %all-gather.6.cloned.1.call-done = bf16[16384,256]{1,0:T(8,128)(2,1)} async-done(((bf16[256,256]{1,0:T(8,128)(2,1)}), bf16[16384,256]{1,0:T(8,128)(2,1)}) %all-gather.6.cloned.1.call-update) | async-done | bytes 8388624 | tf_op jit(solution)/shard_map/all_gather | solution.py:79
  125.3 5.7 %fusion.177 = (bf16[16384,128]{1,0:T(8,128)(2,1)}, bf16[16384,128]{1,0:T(8,128)(2,1)}) fusion(bf16[16384,256]{1,0:T(8,128)(2,1)} %all-gather.6.cloned.1.call-done), kind=kLoop, calls=%fused_computation.271 | loop fusion | bytes 16777216 | tf_op jit(solution)/shard_map/split | solution.py:80
  131.0 6.4 %copy.80 = bf16[16384,128]{0,1:T(8,128)(2,1)} copy(bf16[16384,128]{1,0:T(8,128)(2,1)} %get-tuple-element.510) | data formatting | bytes 8388608 | tf_op jit(solution)/shard_map/while | solution.py:275
  137.4 6.4 %copy.81 = bf16[16384,128]{0,1:T(8,128)(2,1)} copy(bf16[16384,128]{1,0:T(8,128)(2,1)} %get-tuple-element.509) | data formatting | bytes 8388608 | tf_op jit(solution)/shard_map/while | solution.py:275
  143.9 137.3 %while.30 = (s32[]{:T(128)}, f32[2,256]{1,0:T(2,128)S(1)}, f32[2,256]{1,0:T(2,128)S(1)}, f32[256,2,64]{0,2,1:T(8,128)S(1)}, s32[256]{0:T(256)S(1)}, /*index=5*/b...) while((s32[]{:T(128)}, f32[2,256]{1,0:T(2,128)S(1)}, ...), condition=%wide.region_12.13_spmd, body=%wide.region_7.12_spmd.sunk | while | flops 70191104 | bytes 4840789 | solution.py:275
  145.2 2.9 conditional.2
  149.5 2.9 conditional.2
  158.1 2.9 conditional.2
  166.7 2.9 conditional.2
  175.3 2.9 conditional.2
  183.8 2.9 conditional.2
  192.4 2.9 conditional.2
  201.0 2.9 conditional.2
  218.2 2.9 conditional.2
  235.3 2.9 conditional.2
  243.9 2.9 conditional.2
  261.1 2.9 conditional.2
  282.2 4.1 %all-to-all-start.2 = ((bf16[8,256,128]{1,2,0:T(8,128)(2,1)}), bf16[8,256,128]{1,2,0:T(8,128)(2,1)S(1)}, u32[]{:S(2)}, u32[]{:S(2)}) async-start(bf16[8,256,128]{1,2,0:T(8,128)(2,1)} %broadcast_in_dim.78), calls=%async_computation.2 | async-start | bytes 1048576 | tf_op jit(solution)/shard_map/all_to_all | solution.py:17
  286.7 10.0 %all-to-all-done.2 = bf16[8,256,128]{1,2,0:T(8,128)(2,1)S(1)} async-done(((bf16[8,256,128]{1,2,0:T(8,128)(2,1)}), bf16[8,256,128]{1,2,0:T(8,128)(2,1)S(1)}, u32[]{:S(2)}, u32[]{:S(2)}) %all-to-all-start.2) | async-done | bytes 524320 | tf_op jit(solution)/shard_map/all_to_all | solution.py:17
  (535 shorter events, 194.4 us)
Async XLA Ops:
  6.5 25.9 %copy-start = (bf16[2048,128]{1,0:T(8,128)(2,1)S(1)}, bf16[2048,128]{1,0:T(8,128)(2,1)}, u32[]{:S(2)}) copy-start(bf16[2048,128]{1,0:T(8,128)(2,1)} %param.25) | copy-start | bytes 1572868
  6.5 118.8 %all-gather.6.cloned.1.call-start = ((), (), s32[]{:S(2)}) async-start(), calls=%async_computation.3 | async-start | bytes 8519680 | tf_op jit(solution)/shard_map/all_gather | solution.py:79
  7.6 20.5 %copy-start.8 = (f32[2048]{0:T(1024)S(1)}, f32[2048]{0:T(1024)}, u32[]{:S(2)}) copy-start(f32[2048]{0:T(1024)} %param.23) | copy-start | bytes 24580
  27.8 1.0 copy-start.3
  28.1 1.2 copy-start.4
  28.8 2.5 copy-start.13
  28.8 2.5 copy-start.5
  29.3 2.6 copy-start.6
  29.8 2.6 copy-start.12
  31.9 1.2 copy-start.1
  33.6 63.7 %copy-start.11 = (f32[1,128,128]{2,1,0:T(8,128)S(1)}, f32[1,128,128]{2,1,0:T(8,128)}, u32[]{:S(2)}) copy-start(f32[1,128,128]{2,1,0:T(8,128)} %param.29) | copy-start | bytes 196612
  46.6 51.4 %copy-start.9 = (f32[128]{0:T(128)S(1)}, f32[128]{0:T(128)}, u32[]{:S(2)}) copy-start(f32[128]{0:T(128)} %param.30) | copy-start | bytes 1540
  99.0 182.4 %all-to-all-start.1 = ((bf16[8,256,128]{1,2,0:T(8,128)(2,1)}), bf16[8,256,128]{1,2,0:T(8,128)(2,1)S(1)}, u32[]{:S(2)}, u32[]{:S(2)}) async-start(bf16[8,256,128]{1,2,0:T(8,128)(2,1)} %broadcast_in_dim.63), calls=%async_computation.1 | async-start | bytes 1048576 | tf_op jit(solution)/shard_map/all_to_all | solution.py:17
  143.8 137.4 %copy-start.10 = (f32[128]{0:T(128)S(1)}, f32[128]{0:T(128)}, u32[]{:S(2)}) copy-start(f32[128]{0:T(128)} %param.35) | copy-start | bytes 1540
  281.2 5.2 %copy-start.2 = (bf16[1024,256]{1,0:T(8,128)(2,1)S(1)}, bf16[1024,256]{1,0:T(8,128)(2,1)}, u32[]{:S(2)}) copy-start(bf16[1024,256]{1,0:T(8,128)(2,1)} %param.36) | copy-start | bytes 1572868
  281.2 15.5 %copy-start.7 = (bf16[1024,256]{1,0:T(8,128)(2,1)S(1)}, bf16[1024,256]{1,0:T(8,128)(2,1)}, u32[]{:S(2)}) copy-start(bf16[1024,256]{1,0:T(8,128)(2,1)} %param.37) | copy-start | bytes 1572868
  282.2 14.5 %all-to-all-start.2 = ((bf16[8,256,128]{1,2,0:T(8,128)(2,1)}), bf16[8,256,128]{1,2,0:T(8,128)(2,1)S(1)}, u32[]{:S(2)}, u32[]{:S(2)}) async-start(bf16[8,256,128]{1,2,0:T(8,128)(2,1)} %broadcast_in_dim.78), calls=%async_computation.2 | async-start | bytes 1048576 | tf_op jit(solution)/shard_map/all_to_all | solution.py:17
Sparse Core Ops, SparseCore 0:
  30.6 94.6 all-gather.5
where the time goes:
time: 307 us; the launch traced here: 305 us
  local copies, waits for them, and re-layouts  97.8 us (32%)
  blocking collectives  70.2 us (23%)
  waiting for transfers between devices  32.9 us (11%)
  matrix products  32.5 us (11%)
  loops' own time  25.5 us (8%)
  other arithmetic  24.3 us (8%)
  between operations  13.9 us (5%)
  starting transfers between devices  7.63 us (2%)
    all_gather x2, blocking collectives, collected_together(): both, at, found = (lax.all_gather(jnp.concatenate(lines), axis), 0, {})  50.1 us
    dynamic_slice x32, local copies, waits for them, and re-layouts, advance_keys(): lax.dynamic_slice_in_dim(value_part, begin_at, step_rows, 0)  31.7 us
    another operation x1, loops' own time, shards(): folded = lax.fori_loop(0, total_amount // step_rows, advance_keys, initial)  23.1 us
    all_gather x1, waiting for transfers between devices, side_by_side(): out = lax.all_gather(both, axis, axis=dim, tiled=True)  22.9 us
    transpose x32, local copies, waits for them, and re-layouts, compute(): scores = scores + group_gates.T[:, :, None] - key_gates.T[:, None, :]  22.2 us
    slice x32, local copies, waits for them, and re-layouts, advance_keys(): needed = begin_at <= group_index[-1]  20.8 us
    all_to_all x1, blocking collectives, copy_for_each(): lax.all_to_all(jnp.broadcast_to(x[None], (devices, *x.shape)), axis, 0, 0...  20.1 us
    dot_general x32, matrix products, compute(): jnp.einsum('qhd,khd->hqk', group_query, key_rows, preferred_element_type=...  13.9 us
  transfers between devices with their start and end apart: 3, of which 2 were waited for; matrix products, arithmetic and copies ran while one was open for 49% of the time, Pallas kernels for 0%

commit v1 on v0

v1 whole, which is shorter than its diff:
```python
import functools

import jax
import jax.numpy as jnp
from jax import lax
from jax.experimental import pallas as pl
from jax.experimental.pallas import tpu as pltpu
from jax.sharding import Mesh
from jax.sharding import PartitionSpec as P

FD = 64
SP = ("z", "y")
TP = ("x", "c")
EPSILON = 1e-06
LOW = -1e30
SUB = 16
F32 = jnp.float32
BF16 = jnp.bfloat16
MESH = pl.DeviceIdType.MESH
VMEM_LIMIT = 60 * 1024 * 1024


def remote(src, dst, send, recv, device):
    return pltpu.make_async_remote_copy(
        src_ref=src, dst_ref=dst, send_sem=send, recv_sem=recv, device_id=device, device_id_type=MESH
    )


def tp_greet(nx):
    x, c = lax.axis_index("x"), lax.axis_index("c")
    barrier = pltpu.get_barrier_semaphore()
    peers = [{"c": 1 - c}, {"x": lax.rem(x + 1, nx)}, {"x": lax.rem(x + nx - 1, nx)}]
    for peer in peers:
        pl.semaphore_signal(barrier, inc=1, device_id=peer, device_id_type=MESH)
    pl.semaphore_wait(barrier, len(peers))


def tp_gather(nx, slots, send_sem, recv_sem, consume):
    x, c = lax.axis_index("x"), lax.axis_index("c")
    other = 1 - c
    right, left, far = lax.rem(x + 1, nx), lax.rem(x + nx - 1, nx), lax.rem(x + 2, nx)
    half = slots.shape[1] // 2
    me = 2 * x + c
    top, bottom = pl.ds(0, half), pl.ds(half, half)

    def piece(number, p, rows, device):
        ref = slots.at[p] if rows is None else slots.at[p, rows]
        return remote(ref, ref, send_sem.at[number], recv_sem.at[number], device)

    to_right, to_left, to_other = {"x": right}, {"x": left}, {"c": other}
    from_left, from_right, across = 2 * left + c, 2 * right + c, 2 * far + c
    sends = [
        piece(0, me, top, to_right),
        piece(1, me, bottom, to_left),
        piece(2, me, bottom, to_right),
        piece(3, me, top, to_left),
        piece(4, me, None, to_other),
    ]
    for copy in sends:
        copy.start()
    consume(me)

    def forward(number, p, rows, device):
        copy = piece(number, p, rows, device)
        copy.start()
        sends.append(copy)

    piece(0, from_left, top, to_right).wait_recv()
    forward(5, from_left, top, to_right)
    piece(1, from_right, bottom, to_left).wait_recv()
    forward(6, from_right, bottom, to_left)
    piece(4, 2 * x + other, None, to_other).wait_recv()
    consume(2 * x + other)
    piece(2, from_left, bottom, to_right).wait_recv()
    forward(7, from_left, None, to_other)
    piece(3, from_right, top, to_left).wait_recv()
    forward(8, from_right, None, to_other)
    consume(from_left)
    consume(from_right)
    piece(5, across, top, to_right).wait_recv()
    piece(6, across, bottom, to_left).wait_recv()
    forward(9, across, None, to_other)
    piece(7, 2 * left + other, None, to_other).wait_recv()
    consume(2 * left + other)
    piece(8, 2 * right + other, None, to_other).wait_recv()
    consume(2 * right + other)
    consume(across)
    piece(9, 2 * far + other, None, to_other).wait_recv()
    consume(2 * far + other)
    for copy in sends:
        copy.wait_send()


def project_kernel(
    nx, tokens_ref, gain_ref, *refs
):
    weights, out_ref = refs[:6], refs[6]
    slots, held, total, squares, local_sem, weight_sem, send_sem, recv_sem = refs[7:]
    x, c = lax.axis_index("x"), lax.axis_index("c")
    own = pltpu.make_async_copy(tokens_ref, slots.at[2 * x + c], local_sem)
    own.start()
    width = weights[0].shape[1]
    loads = [
        pltpu.make_async_copy(ref, held.at[:, pl.ds(n * width, width)], weight_sem.at[n])
        for n, ref in enumerate(weights)
    ]
    for load in loads:
        load.start()
    total[...] = jnp.zeros_like(total)
    squares[...] = jnp.zeros_like(squares)
    tp_greet(nx)
    own.wait()
    features = tokens_ref.shape[1]
    waited = []

    def consume(p):
        if not waited:
            for load in loads:
                load.wait()
            waited.append(True)
        wide = slots[p].astype(F32)
        squared = wide * wide
        folded = squared[:, :128]
        for k in range(1, features // 128):
            folded = folded + squared[:, k * 128 : (k + 1) * 128]
        squares[...] += folded
        scaled = (wide * gain_ref[p]).astype(BF16)
        rows = pl.ds(pl.multiple_of(p * features, features), features)
        total[...] += jnp.dot(scaled, held[rows, :], preferred_element_type=F32)

    tp_gather(nx, slots, send_sem, recv_sem, consume)
    mean = jnp.sum(squares[...], axis=1, keepdims=True) / held.shape[0]
    inverse = lax.rsqrt(mean + EPSILON)
    out_ref[...] = (total[...] * inverse).astype(BF16)


def output_kernel(nx, rows_ref, recur_ref, attend_ref, out_ref, slots, held, total, local_sem, weight_sem, send_sem, recv_sem):
    x, c = lax.axis_index("x"), lax.axis_index("c")
    own = pltpu.make_async_copy(rows_ref, slots.at[2 * x + c], local_sem)
    own.start()
    depth = rows_ref.shape[1] // 2
    pieces = 2 * nx
    loads = []
    for n in range(pieces):
        for k, ref in enumerate((recur_ref, attend_ref)):
            loads.append(
                pltpu.make_async_copy(
                    ref.at[pl.ds(n * depth, depth)], held.at[n, pl.ds(k * depth, depth)], weight_sem.at[2 * n + k]
                )
            )
    for load in loads:
        load.start()
    total[...] = jnp.zeros_like(total)
    tp_greet(nx)
    own.wait()
    waited = []

    def consume(p):
        if not waited:
            for load in loads:
                load.wait()
            waited.append(True)
        total[...] += jnp.dot(slots[p], held[p], preferred_element_type=F32)

    tp_gather(nx, slots, send_sem, recv_sem, consume)
    out_ref[...] = total[...].astype(BF16)


def thirds(value):
    first = value.astype(BF16)
    rest = value - first.astype(F32)
    second = rest.astype(BF16)
    third = (rest - second.astype(F32)).astype(BF16)
    return first, second, third


def whole(first, second, third):
    return first.astype(F32) + second.astype(F32) + third.astype(F32)


def padded_thirds(rows, height):
    parts = [part.astype(F32) for row in rows for part in thirds(row)]
    parts.append(jnp.zeros((height - len(parts), rows[0].shape[1]), F32))
    return jnp.concatenate(parts, axis=0).astype(BF16)


def nt(left, right):
    return lax.dot_general(left, right, (((1,), (1,)), ((), ())), preferred_element_type=F32)


def middle_kernel(
    nz,
    ny,
    proj_ref,
    floor_ref,
    decay_ref,
    start_ref,
    recur_gain_ref,
    gate_ref,
    attend_gain_ref,
    out_ref,
    kbuf,
    vbuf,
    qbuf,
    sbuf,
    tbuf,
    obuf,
    rbuf,
    acc,
    top,
    bias,
    kv_send,
    kv_recv,
    q_send,
    q_recv,
    t_send,
    t_recv,
    o_send,
    o_recv,
):
    z, y = lax.axis_index("z"), lax.axis_index("y")
    height = proj_ref.shape[0]
    row_at = z * ny * height

    def gates(zq, yq):
        at = pl.multiple_of((zq * ny + yq) * height, height)
        return gate_ref[:, pl.ds(at, height)]

    barrier = pltpu.get_barrier_semaphore()
    for step in (1, ny - 1):
        pl.semaphore_signal(barrier, inc=1, device_id={"y": lax.rem(y + step, ny)}, device_id_type=MESH)
    for step in range(1, nz):
        pl.semaphore_signal(barrier, inc=1, device_id={"z": lax.rem(z + step, nz)}, device_id_type=MESH)

    kbuf[y] = proj_ref[:, 512:640]
    values_t = jnp.transpose(proj_ref[:, 640:768].astype(F32))
    vbuf[y] = values_t.astype(BF16)
    query_t = jnp.transpose(proj_ref[:, 384:512].astype(F32) * (FD**-0.5))
    qbuf[z] = query_t.astype(BF16)
    pl.semaphore_wait(barrier, nz + 1)

    y_next, y_last = {"y": lax.rem(y + 1, ny)}, {"y": lax.rem(y + ny - 1, ny)}
    z_next, z_last = {"z": lax.rem(z + 1, nz)}, {"z": lax.rem(z + nz - 1, nz)}
    kv = (kbuf, vbuf, sbuf)

    def y_copy(way, unit, slot, step):
        device = y_next if way == 0 else y_last
        ref = kv[unit].at[slot]
        return remote(ref, ref, kv_send.at[way, unit, step], kv_recv.at[way, unit, step], device)

    def z_copy(way, slot, step):
        device = z_next if way == 0 else z_last
        ref = qbuf.at[slot]
        return remote(ref, ref, q_send.at[way, step], q_recv.at[way, step], device)

    def y_units(way, step):
        if 2 * step < ny:
            return (0, 1, 2)
        return (0, 2) if way == 0 else (1,)

    def y_slot(way, step):
        return lax.rem(y + ny - step, ny) if way == 0 else lax.rem(y + step, ny)

    def z_slot(way, step):
        return lax.rem(z + nz - step, nz) if way == 0 else lax.rem(z + step, nz)

    started = []

    def begin(copy):
        copy.start()
        started.append(copy)

    def y_begin(step, units):
        for unit in units:
            for way in (0, 1):
                if unit in y_units(way, step):
                    begin(y_copy(way, unit, y_slot(way, step - 1), step - 1))

    def z_ways(step):
        return (0, 1) if 2 * step < nz else (0,)

    y_begin(1, (0, 1))
    for way in z_ways(1):
        begin(z_copy(way, z, 0))

    queries = proj_ref[:, 0:128].astype(F32)
    forget = proj_ref[:, 128:256].astype(F32)
    values = proj_ref[:, 256:384]
    inflow = (1.0 - floor_ref[...]) / (1.0 + jnp.exp(forget))
    extra = jnp.transpose(jnp.broadcast_to(decay_ref[...], (128, height)))
    decays = jnp.log1p(-inflow) - extra
    rows_i = lax.broadcasted_iota(jnp.int32, (height, height), 0)
    cols_i = lax.broadcasted_iota(jnp.int32, (height, height), 1)
    lower = jnp.where(cols_i <= rows_i, 1.0, 0.0).astype(BF16)
    sums = jnp.zeros((height, 128), F32)
    for part in thirds(decays):
        sums = sums + jnp.dot(lower, part, preferred_element_type=F32)
    ending = sums[height - 1 : height, :]
    kept = (inflow * jnp.exp(ending - sums)).astype(BF16)
    values_rt = jnp.transpose(values.astype(F32)).astype(BF16)
    sbuf[y] = jnp.concatenate(
        [jnp.dot(values_rt, kept, preferred_element_type=F32).astype(BF16), padded_thirds([ending], 16)], axis=0
    )
    y_begin(1, (2,))
    mixing = []
    for at in range(0, height, SUB):
        reach = 128 if at + SUB <= 128 else height
        base = sums[at - 1 : at, :] if at else jnp.zeros((1, 128), F32)
        near = queries[at : at + SUB] * jnp.exp(sums[at : at + SUB] - base)
        past = inflow[:reach] * jnp.exp(jnp.minimum(base - sums[:reach], 60.0))
        piece = nt(near.astype(BF16), past.astype(BF16))
        if reach < height:
            piece = jnp.concatenate([piece, jnp.zeros((SUB, height - reach), F32)], axis=1)
        mixing.append(piece)
    mixing = jnp.where(cols_i <= rows_i, jnp.concatenate(mixing, axis=0), 0.0)
    local_out = jnp.dot(mixing.astype(BF16), values, preferred_element_type=F32)
    carried_query = (queries * jnp.exp(sums)).astype(BF16)

    reference_gate = gates(z, ny - 1)[:, height - 1 : height]
    for slot in range(ny):
        relative = reference_gate - gates(z, slot)
        for head in range(2):
            bias[slot, head] = jnp.transpose(jnp.broadcast_to(relative[head : head + 1], (128, height)))
    top[...] = jnp.full(top.shape, LOW, F32)
    acc[...] = jnp.zeros_like(acc)
    ones = jnp.ones((16, height), BF16)
    blank = jnp.zeros((FD, height), BF16)

    def update(zq, yk, own):
        keys = kbuf[yk]
        for head in range(2):
            part = qbuf[zq, head * FD : (head + 1) * FD]
            split = jnp.concatenate([part, blank] if head == 0 else [blank, part], axis=0)
            scores = jnp.dot(keys, split, preferred_element_type=F32)
            shift = bias[yk, head]
            scores = scores + jnp.concatenate([shift] * (height // 128), axis=1)
            if own:
                scores = jnp.where(rows_i <= cols_i, scores, LOW)
            old = top[zq, head]
            new = jnp.maximum(old, jnp.max(scores, axis=0, keepdims=True))
            weights = jnp.exp(scores - new[0:1])
            rescale = jnp.exp(old - new)[0:1]
            top[zq, head] = new
            left = jnp.concatenate([vbuf[yk, head * FD : (head + 1) * FD], ones], axis=0)
            acc[zq, head] = acc[zq, head] * rescale + jnp.dot(
                left, weights.astype(BF16), preferred_element_type=F32
            )

    update(z, y, True)

    def visit(oq, ok):
        zq, yk = lax.rem(z + oq + nz, nz), lax.rem(y + ok + ny, ny)
        needed = (zq > z) | ((zq == z) & (yk < y))

        @pl.when(needed)
        def _():
            update(zq, yk, False)

    for step in range(1, ny // 2 + 1):
        for unit in (0, 1, 2):
            for way in (0, 1):
                if unit in y_units(way, step):
                    slot = y_slot(way, step)
                    y_copy(way, unit, slot, step - 1).wait_recv()
                    if unit in y_units(way, step + 1) and step < ny // 2:
                        begin(y_copy(way, unit, slot, step))
        for way in z_ways(step):
            slot = z_slot(way, step)
            z_copy(way, slot, step - 1).wait_recv()
            if step < nz // 2 and way in z_ways(step + 1):
                begin(z_copy(way, slot, step))
        if step < ny // 2:

            def ring(n, carry, step=step):
                side, r = n // (2 * step), n % (2 * step)
                oq = jnp.where(side == 0, r - step, jnp.where(side == 1, step, jnp.where(side == 2, step - r, -step)))
                ok = jnp.where(side == 0, -step, jnp.where(side == 1, r - step, jnp.where(side == 2, step, step - r)))
                visit(oq, ok)
                return carry

            lax.fori_loop(0, 8 * step, ring, 0)
        else:
            state = jnp.zeros((128, 128), F32)
            inside = state
            log_all = jnp.zeros((1, 128), F32)
            log_before = log_all
            for slot in range(ny):
                block = sbuf[slot].astype(F32)
                log_own = block[128:129] + block[129:130] + block[130:131]
                state = state * jnp.exp(log_own) + block[:128]
                log_all = log_all + log_own
                inside = jnp.where(slot < y, state, inside)
                log_before = jnp.where(slot < y, log_all, log_before)
            tbuf[z] = jnp.concatenate([state.astype(BF16), padded_thirds([log_all], 16)], axis=0)

            def t_copy(slot, target):
                ref = tbuf.at[slot]
                return remote(ref, ref, t_send.at[target], t_recv.at[slot], {"z": target})

            @pl.loop(z + 1, nz)
            def _(target):
                t_copy(z, target).start()

            def last(n, carry, step=step):
                oq = jnp.where(n < 2 * step, n - step + 1, step)
                ok = jnp.where(n < 2 * step, step, n - 3 * step + 1)
                visit(oq, ok)
                return carry

            lax.fori_loop(0, 4 * step - 1, last, 0)

    def o_copy(source, slot, target):
        return remote(obuf.at[slot], rbuf.at[source], o_send.at[slot], o_recv.at[source], {"z": target})

    def logs_of(zq):
        shift = gates(zq, y) - reference_gate
        return [
            top[zq, head][0:1] + jnp.log(acc[zq, head][FD : FD + 1]) + shift[head : head + 1] for head in range(2)
        ]

    def rows_of(zq):
        return [acc[zq, head][:FD] / acc[zq, head][FD : FD + 1] for head in range(2)]

    @pl.loop(z + 1, nz)
    def _(target):
        obuf[target] = jnp.concatenate(
            [part.astype(BF16) for part in rows_of(target)] + [padded_thirds(logs_of(target), 16)], axis=0
        )
        o_copy(z, target, target).start()

    def take(slot, state):
        t_copy(slot, z).wait_recv()
        block = tbuf[slot].astype(F32)
        log_own = block[128:129] + block[129:130] + block[130:131]
        return state * jnp.exp(log_own) + block[:128]

    arriving = lax.fori_loop(0, z, take, jnp.transpose(start_ref[...]))
    arriving = arriving * jnp.exp(log_before) + inside
    rec_out = local_out + nt(carried_query, arriving.astype(BF16))
    mean = jnp.mean(rec_out * rec_out, axis=1, keepdims=True)
    out_ref[:, 0:128] = (rec_out * lax.rsqrt(mean + EPSILON) * recur_gain_ref[...]).astype(BF16)

    def merge(slot, carry):
        o_copy(slot, slot, z).wait_recv()
        block = rbuf[slot].astype(F32)
        merged = []
        for head in range(2):
            best, amount, rows = carry[3 * head : 3 * head + 3]
            at = 2 * FD + 3 * head
            log = block[at : at + 1] + block[at + 1 : at + 2] + block[at + 2 : at + 3]
            new = jnp.maximum(best, log)
            keep, add = jnp.exp(best - new), jnp.exp(log - new)
            merged += [new, amount * keep + add, rows * keep + block[head * FD : (head + 1) * FD] * add]
        return tuple(merged)

    own_logs, own_rows = logs_of(z), rows_of(z)
    start = []
    for head in range(2):
        start += [own_logs[head], jnp.ones((1, height), F32), own_rows[head]]
    merged = lax.fori_loop(0, z, merge, tuple(start))
    normed = []
    for head in range(2):
        rows = merged[3 * head + 2] / merged[3 * head + 1]
        mean = jnp.mean(rows * rows, axis=0, keepdims=True)
        normed.append(rows * lax.rsqrt(mean + EPSILON))
    att_rows = jnp.transpose(jnp.concatenate(normed, axis=0))
    out_ref[:, 128:256] = (att_rows * attend_gain_ref[...]).astype(BF16)

    for copy in started:
        copy.wait_send()

    @pl.loop(z + 1, nz)
    def _(target):
        t_copy(z, target).wait_send()
        o_copy(z, target, target).wait_send()


VM = pl.BlockSpec(memory_space=pltpu.VMEM)
ANY = pl.BlockSpec(memory_space=pl.ANY)
DMA = pltpu.SemaphoreType.DMA


def params(number):
    return pltpu.CompilerParams(collective_id=number, has_side_effects=True, vmem_limit_bytes=VMEM_LIMIT)


def project(nx, tokens, norm_gain, weights):
    height, features = tokens.shape
    model = norm_gain.shape[0]
    width = sum(weight.shape[1] for weight in weights)
    return pl.pallas_call(
        functools.partial(project_kernel, nx),
        out_shape=jax.ShapeDtypeStruct((height, width), BF16),
        in_specs=[ANY, VM] + [ANY] * 6,
        out_specs=VM,
        scratch_shapes=[
            pltpu.VMEM((2 * nx, height, features), BF16),
            pltpu.VMEM((model, width), BF16),
            pltpu.VMEM((height, width), F32),
            pltpu.VMEM((height, 128), F32),
            DMA,
            DMA((6,)),
            DMA((10,)),
            DMA((10,)),
        ],
        compiler_params=params(0),
        name="project",
    )(tokens, norm_gain.reshape(2 * nx, 1, features), *weights)


def middle(nz, ny, projected, gate_floor, extra_decay, start_state, recur_gain, gate_cache, attend_gain):
    height = projected.shape[0]
    return pl.pallas_call(
        functools.partial(middle_kernel, nz, ny),
        out_shape=jax.ShapeDtypeStruct((height, 256), BF16),
        in_specs=[VM] * 7,
        out_specs=VM,
        scratch_shapes=[
            pltpu.VMEM((ny, height, 128), BF16),
            pltpu.VMEM((ny, 128, height), BF16),
            pltpu.VMEM((nz, 128, height), BF16),
            pltpu.VMEM((ny, 144, 128), BF16),
            pltpu.VMEM((nz, 144, 128), BF16),
            pltpu.VMEM((nz, 144, height), BF16),
            pltpu.VMEM((nz, 144, height), BF16),
            pltpu.VMEM((nz, 2, FD + 16, height), F32),
            pltpu.VMEM((nz, 2, 8, height), F32),
            pltpu.VMEM((ny, 2, height, 128), F32),
            DMA((2, 3, ny // 2)),
            DMA((2, 3, ny // 2)),
            DMA((2, nz // 2)),
            DMA((2, nz // 2)),
            DMA((nz,)),
            DMA((nz,)),
            DMA((nz,)),
            DMA((nz,)),
        ],
        compiler_params=params(1),
        name="middle",
    )(
        projected,
        gate_floor.reshape(1, -1),
        extra_decay.reshape(1, -1),
        start_state.reshape(128, 128),
        recur_gain.reshape(1, -1),
        gate_cache.T,
        attend_gain.reshape(1, -1),
    )


def output(nx, rows, recur_output, attend_output):
    height = rows.shape[0]
    width = recur_output.shape[1]
    return pl.pallas_call(
        functools.partial(output_kernel, nx),
        out_shape=jax.ShapeDtypeStruct((height, width), BF16),
        in_specs=[ANY] * 3,
        out_specs=VM,
        scratch_shapes=[
            pltpu.VMEM((2 * nx, height, 256), BF16),
            pltpu.VMEM((2 * nx, 256, width), BF16),
            pltpu.VMEM((height, width), F32),
            DMA,
            DMA((4 * nx,)),
            DMA((10,)),
            DMA((10,)),
        ],
        compiler_params=params(2),
        name="output",
    )(rows, recur_output, attend_output)


def shards(
    sizes,
    tokens,
    norm_gain,
    recur_query,
    recur_forget,
    recur_value,
    gate_floor,
    extra_decay,
    start_state,
    recur_gain,
    attend_query,
    attend_key,
    attend_value,
    gate_cache,
    attend_gain,
    recur_output,
    attend_output,
):
    nz, ny, nx = sizes
    weights = (recur_query, recur_forget, recur_value, attend_query, attend_key, attend_value)
    projected = project(nx, tokens, norm_gain, weights)
    rows = middle(nz, ny, projected, gate_floor, extra_decay, start_state, recur_gain, gate_cache, attend_gain)
    return output(nx, rows, recur_output, attend_output)


def solution(mesh):
    sizes = (8, 8, 4)
    finer = Mesh(mesh.devices.reshape(*sizes, 2), ("z", "y", "x", "c"))
    return jax.shard_map(
        functools.partial(shards, sizes),
        mesh=finer,
        in_specs=(
            P(SP, TP),
            P(),
            P(None, TP),
            P(None, TP),
            P(None, TP),
            P(TP),
            P(SP, TP),
            P(TP, None, None),
            P(TP),
            P(None, TP),
            P(None, TP),
            P(None, TP),
            P(None, TP),
            P(TP),
            P(None, TP),
            P(None, TP),
        ),
        out_specs=P(SP, TP),
        check_vma=False,
    )
```

time: 307 us -> 95.8 us (0.31)
  the two profiles are of different devices: /device:TPU:496 before, /device:TPU:1 now
where the time goes in v1:
time: 95.8 us; the launch traced here: 94.5 us
  Pallas kernels  92.9 us (97%)
  local copies, waits for them, and re-layouts  1.57 us (2%)
    pallas_call x1, Pallas kernels, middle(): pl.pallas_call(functools.partial(middle_kernel, nz, ny), out_shape=jax.Sh...  61.5 us
    pallas_call x1, Pallas kernels, project(): pl.pallas_call(functools.partial(project_kernel, nx), out_shape=jax.Shape...  18.9 us
    pallas_call x1, Pallas kernels, output(): pl.pallas_call(functools.partial(output_kernel, nx), out_shape=jax.ShapeD...  12.5 us

profile of v1, /device:TPU:1, one launch (start us, length us, event | category | flops | bytes accessed | tf_op | source)
XLA Modules:
  0.0 94.5 jit_solution(325154987227917491)
XLA Ops:
  0.0 18.9 %project.1.proj_ref = bf16[256,768]{1,0:T(8,128)(2,1)} custom-call(bf16[256,256]{1,0:T(8,128)(2,1)} %tokens_ref.1, f32[8,1,256]{2,1,0:T(1,128)} %bitcast.9, bf16[2048,128]{1,0:T(8,128)(2,1)} %refs_0_.1, bf16[2048,128]{1,0:T(8,128)(2,1)} %refs_1_.1, bf16[2048,128]{1,0:T(8,128)(2,1)} %refs_2_.1, bf16[2048,128]{1,0:T(8,128)(2,1)} %refs_3_.1, ...), custom_call_target="tpu_custom_call" | custom-call | tf_op jit(solution)/shard_map/project/pallas_call | solution.py:491
  18.9 61.5 %middle.1.rows_ref = bf16[256,256]{1,0:T(8,128)(2,1)} custom-call(bf16[256,768]{1,0:T(8,128)(2,1)} %project.1.proj_ref, f32[1,128]{1,0:T(1,128)} %bitcast.11, f32[1,256]{1,0:T(1,128)} %bitcast.10, f32[128,128]{1,0:T(8,128)} %bitcast.8, f32[1,128]{1,0:T(1,128)} %bitcast.12, f32[2,16384]{1,0:T(2,128)} %bitcast.7, f32[1,128]{1,0:T(1,128)} %bitcast.13), custom_call_target="tpu_custom_call" | custom-call | tf_op jit(solution)/shard_map/middle/pallas_call | solution.py:513
  80.4 12.5 %output.1 = bf16[256,256]{1,0:T(8,128)(2,1)} custom-call(bf16[256,256]{1,0:T(8,128)(2,1)} %middle.1.rows_ref, bf16[1024,256]{1,0:T(8,128)(2,1)} %recur_ref.1, bf16[1024,256]{1,0:T(8,128)(2,1)} %attend_ref.1), custom_call_target="tpu_custom_call" | custom-call | tf_op jit(solution)/shard_map/output/pallas_call | solution.py:554
  92.9 1.6 %copy.18 = bf16[256,256]{1,0:T(8,128)(2,1)} copy(bf16[256,256]{1,0:T(8,128)(2,1)} %output.1) | data formatting | bytes 262144

commit v2 on v1

--- a/solution.py
+++ b/solution.py
@@ -14,6 +14,7 @@
 EPSILON = 1e-06
 LOW = -1e30
 SUB = 16
+LANES = 2
 F32 = jnp.float32
 BF16 = jnp.bfloat16
 MESH = pl.DeviceIdType.MESH
@@ -209,6 +210,11 @@
     acc,
     top,
     bias,
+    score_s,
+    weight_s,
+    top_s,
+    scale_s,
+    scale_w,
     kv_send,
     kv_recv,
     q_send,
@@ -348,13 +354,85 @@
 
     update(z, y, True)
 
-    def visit(oq, ok):
-        zq, yk = lax.rem(z + oq + nz, nz), lax.rem(y + ok + ny, ny)
-        needed = (zq > z) | ((zq == z) & (yk < y))
-
-        @pl.when(needed)
-        def _():
-            update(zq, yk, False)
+    def pipeline(count, place):
+        def at(number):
+            return place(jnp.clip(number, 0, count - 1))
+
+        def scores_of(number, lane):
+            zq, yk = at(number)
+            keys = kbuf[yk]
+            later = jnp.where((zq == z) & (yk > y), LOW, 0.0)
+            for head in range(2):
+                part = qbuf[zq, head * FD : (head + 1) * FD]
+                split = jnp.concatenate([part, blank] if head == 0 else [blank, part], axis=0)
+                scores = jnp.dot(keys, split, preferred_element_type=F32)
+                shift = bias[yk, head] + later
+                scores = scores + jnp.concatenate([shift] * (height // 128), axis=1)
+                old = top[zq, head]
+                new = jnp.maximum(old, jnp.max(scores, axis=0, keepdims=True))
+                score_s[lane, head] = scores
+                top[zq, head] = new
+                top_s[lane, head] = new
+                scale_s[lane, head] = jnp.exp(old - new)
+
+        def weights_of(lane):
+            for head in range(2):
+                weight_s[lane, head] = jnp.exp(score_s[lane, head] - top_s[lane, head][0:1]).astype(BF16)
+                scale_w[lane, head] = scale_s[lane, head]
+
+        def sums_of(number, lane):
+            zq, yk = at(number)
+            for head in range(2):
+                left = jnp.concatenate([vbuf[yk, head * FD : (head + 1) * FD], ones], axis=0)
+                acc[zq, head] = acc[zq, head] * scale_w[lane, head][0:1] + jnp.dot(
+                    left, weight_s[lane, head], preferred_element_type=F32
+                )
+
+        weight_s[...] = jnp.zeros_like(weight_s)
+        scale_w[...] = jnp.ones_like(scale_w)
+        for lane in range(LANES):
+            scores_of(lane, lane)
+        rounds = (count + LANES - 1) // LANES
+
+        def turn(n, carry):
+            for lane in range(LANES):
+                number = n * LANES + lane
+                sums_of(number - LANES, lane)
+                weights_of(lane)
+                scores_of(number + LANES, lane)
+            return carry
+
+        lax.fori_loop(0, rounds, turn, 0)
+        for lane in range(LANES):
+            number = (rounds - 1) * LANES + lane
+
+            @pl.when(number < count)
+            def _(number=number, lane=lane):
+                sums_of(number, lane)
+
+    def fold(step):
+        last = 2 * step == nz
+        back = min(step, nz // 2 - 1)
+        ahead = jnp.minimum(step, nz - 1 - z) + 1
+        behind = jnp.maximum(back - z, 0)
+        fresh = 1 if last else 2
+        first = (ahead + behind) * fresh
+        one = jnp.where(z + step <= nz - 1, 1, 0)
+        two = 0 if last else jnp.where(z <= step - 1, 1, 0)
+        known = 2 * step - 1
+
+        def place(number):
+            which = number // fresh
+            oq = jnp.where(which < ahead, which, nz - back + which - ahead)
+            ok = step if last else (number % 2) * (2 * step) - step
+            rest = jnp.maximum(number - first, 0)
+            second = rest // known
+            oq_new = jnp.where((second == 0) & (one == 1), step, nz - step)
+            ok_new = rest % known - (step - 1)
+            old = number < first
+            return z + jnp.where(old, oq, oq_new), lax.rem(y + jnp.where(old, ok, ok_new) + ny, ny)
+
+        pipeline(first + (one + two) * known, place)
 
     for step in range(1, ny // 2 + 1):
         for unit in (0, 1, 2):
@@ -370,15 +448,7 @@
             if step < nz // 2 and way in z_ways(step + 1):
                 begin(z_copy(way, slot, step))
         if step < ny // 2:
-
-            def ring(n, carry, step=step):
-                side, r = n // (2 * step), n % (2 * step)
-                oq = jnp.where(side == 0, r - step, jnp.where(side == 1, step, jnp.where(side == 2, step - r, -step)))
-                ok = jnp.where(side == 0, -step, jnp.where(side == 1, r - step, jnp.where(side == 2, step, step - r)))
-                visit(oq, ok)
-                return carry
-
-            lax.fori_loop(0, 8 * step, ring, 0)
+            fold(step)
         else:
             state = jnp.zeros((128, 128), F32)
             inside = state
@@ -401,13 +471,7 @@
             def _(target):
                 t_copy(z, target).start()
 
-            def last(n, carry, step=step):
-                oq = jnp.where(n < 2 * step, n - step + 1, step)
-                ok = jnp.where(n < 2 * step, step, n - 3 * step + 1)
-                visit(oq, ok)
-                return carry
-
-            lax.fori_loop(0, 4 * step - 1, last, 0)
+            fold(step)
 
     def o_copy(source, slot, target):
         return remote(obuf.at[slot], rbuf.at[source], o_send.at[slot], o_recv.at[source], {"z": target})
@@ -526,6 +590,11 @@
             pltpu.VMEM((nz, 2, FD + 16, height), F32),
             pltpu.VMEM((nz, 2, 8, height), F32),
             pltpu.VMEM((ny, 2, height, 128), F32),
+            pltpu.VMEM((LANES, 2, height, height), F32),
+            pltpu.VMEM((LANES, 2, height, height), BF16),
+            pltpu.VMEM((LANES, 2, 8, height), F32),
+            pltpu.VMEM((LANES, 2, 8, height), F32),
+            pltpu.VMEM((LANES, 2, 8, height), F32),
             DMA((2, 3, ny // 2)),
             DMA((2, 3, ny // 2)),
             DMA((2, nz // 2)),

time: 95.8 us -> 81.9 us (0.85); the launches traced: 94.5 us -> 81.6 us
  Pallas kernels: 92.9 us -> 80 us
    pallas_call x1, Pallas kernels: 61.5 us -> 48.6 us  [middle(): pl.pallas_call(functools.partial(middle_kernel, nz, ny), out_shape=jax.Sh...]
where the time goes in v2:
time: 81.9 us; the launch traced here: 81.6 us
  Pallas kernels  80 us (98%)
  local copies, waits for them, and re-layouts  1.57 us (2%)
    pallas_call x1, Pallas kernels, middle(): pl.pallas_call(functools.partial(middle_kernel, nz, ny), out_shape=jax.Sh...  48.6 us
    pallas_call x1, Pallas kernels, project(): pl.pallas_call(functools.partial(project_kernel, nx), out_shape=jax.Shape...  18.9 us
    pallas_call x1, Pallas kernels, output(): pl.pallas_call(functools.partial(output_kernel, nx), out_shape=jax.ShapeD...  12.5 us

profile of v2, /device:TPU:1, one launch (start us, length us, event | category | flops | bytes accessed | tf_op | source)
XLA Modules:
  0.0 81.6 jit_solution(1235897210273771168)
XLA Ops:
  0.0 18.9 %project.1.proj_ref = bf16[256,768]{1,0:T(8,128)(2,1)} custom-call(bf16[256,256]{1,0:T(8,128)(2,1)} %tokens_ref.1, f32[8,1,256]{2,1,0:T(1,128)} %bitcast.9, bf16[2048,128]{1,0:T(8,128)(2,1)} %refs_0_.1, bf16[2048,128]{1,0:T(8,128)(2,1)} %refs_1_.1, bf16[2048,128]{1,0:T(8,128)(2,1)} %refs_2_.1, bf16[2048,128]{1,0:T(8,128)(2,1)} %refs_3_.1, ...), custom_call_target="tpu_custom_call" | custom-call | tf_op jit(solution)/shard_map/project/pallas_call | solution.py:555
  18.9 48.6 %middle.1.rows_ref = bf16[256,256]{1,0:T(8,128)(2,1)} custom-call(bf16[256,768]{1,0:T(8,128)(2,1)} %project.1.proj_ref, f32[1,128]{1,0:T(1,128)} %bitcast.11, f32[1,256]{1,0:T(1,128)} %bitcast.10, f32[128,128]{1,0:T(8,128)} %bitcast.8, f32[1,128]{1,0:T(1,128)} %bitcast.12, f32[2,16384]{1,0:T(2,128)} %bitcast.7, f32[1,128]{1,0:T(1,128)} %bitcast.13), custom_call_target="tpu_custom_call" | custom-call | tf_op jit(solution)/shard_map/middle/pallas_call | solution.py:577
  67.5 12.5 %output.1 = bf16[256,256]{1,0:T(8,128)(2,1)} custom-call(bf16[256,256]{1,0:T(8,128)(2,1)} %middle.1.rows_ref, bf16[1024,256]{1,0:T(8,128)(2,1)} %recur_ref.1, bf16[1024,256]{1,0:T(8,128)(2,1)} %attend_ref.1), custom_call_target="tpu_custom_call" | custom-call | tf_op jit(solution)/shard_map/output/pallas_call | solution.py:623
  80.0 1.6 %copy.18 = bf16[256,256]{1,0:T(8,128)(2,1)} copy(bf16[256,256]{1,0:T(8,128)(2,1)} %output.1) | data formatting | bytes 262144

commit v3 on v2

--- a/solution.py
+++ b/solution.py
@@ -190,8 +190,7 @@
 
 
 def middle_kernel(
-    nz,
-    ny,
+    size,
     proj_ref,
     floor_ref,
     decay_ref,
@@ -203,8 +202,14 @@
     kbuf,
     vbuf,
     qbuf,
-    sbuf,
-    tbuf,
+    slice_out,
+    slice_in,
+    total_in,
+    state_out,
+    state_in,
+    start_t,
+    prefix,
+    log_prefix,
     obuf,
     rbuf,
     acc,
@@ -219,56 +224,72 @@
     kv_recv,
     q_send,
     q_recv,
+    s_send,
+    s_recv,
     t_send,
     t_recv,
+    u_send,
+    u_recv,
     o_send,
     o_recv,
 ):
-    z, y = lax.axis_index("z"), lax.axis_index("y")
+    z, y, c = lax.axis_index("z"), lax.axis_index("y"), lax.axis_index("c")
     height = proj_ref.shape[0]
-    row_at = z * ny * height
-
-    def gates(zq, yq):
-        at = pl.multiple_of((zq * ny + yq) * height, height)
-        return gate_ref[:, pl.ds(at, height)]
+    mine = 1 - c
+    a, b = mine * y + c * z, mine * z + c * y
+
+    def on_a(index):
+        return {"y": mine * index + c * y, "z": mine * z + c * index}
+
+    def on_b(index):
+        return {"z": mine * index + c * z, "y": mine * y + c * index}
+
+    def gates(block):
+        return gate_ref[:, pl.ds(pl.multiple_of(block * height, height), height)]
+
+    def key_gates(index):
+        return gates(mine * (z * size + index) + c * (index * size + y))
+
+    def query_gates(index):
+        return gates(mine * (index * size + y) + c * (z * size + index))
+
+    def shifted(place, offset):
+        return lax.rem(place + offset + size, size)
 
     barrier = pltpu.get_barrier_semaphore()
-    for step in (1, ny - 1):
-        pl.semaphore_signal(barrier, inc=1, device_id={"y": lax.rem(y + step, ny)}, device_id_type=MESH)
-    for step in range(1, nz):
-        pl.semaphore_signal(barrier, inc=1, device_id={"z": lax.rem(z + step, nz)}, device_id_type=MESH)
-
-    kbuf[y] = proj_ref[:, 512:640]
+    for step in range(1, size):
+        for device in ({"y": shifted(y, step)}, {"z": shifted(z, step)}):
+            pl.semaphore_signal(barrier, inc=1, device_id=device, device_id_type=MESH)
+
+    kbuf[a] = proj_ref[:, 512:640]
     values_t = jnp.transpose(proj_ref[:, 640:768].astype(F32))
-    vbuf[y] = values_t.astype(BF16)
+    vbuf[a] = values_t.astype(BF16)
     query_t = jnp.transpose(proj_ref[:, 384:512].astype(F32) * (FD**-0.5))
-    qbuf[z] = query_t.astype(BF16)
-    pl.semaphore_wait(barrier, nz + 1)
-
-    y_next, y_last = {"y": lax.rem(y + 1, ny)}, {"y": lax.rem(y + ny - 1, ny)}
-    z_next, z_last = {"z": lax.rem(z + 1, nz)}, {"z": lax.rem(z + nz - 1, nz)}
-    kv = (kbuf, vbuf, sbuf)
-
-    def y_copy(way, unit, slot, step):
-        device = y_next if way == 0 else y_last
+    qbuf[b] = query_t.astype(BF16)
+    pl.semaphore_wait(barrier, 2 * (size - 1))
+
+    kv = (kbuf, vbuf)
+
+    def a_copy(way, unit, slot, step):
         ref = kv[unit].at[slot]
-        return remote(ref, ref, kv_send.at[way, unit, step], kv_recv.at[way, unit, step], device)
-
-    def z_copy(way, slot, step):
-        device = z_next if way == 0 else z_last
+        target = on_a(shifted(a, 1 if way == 0 else -1))
+        return remote(ref, ref, kv_send.at[way, unit, step], kv_recv.at[way, unit, step], target)
+
+    def b_copy(way, slot, step):
         ref = qbuf.at[slot]
-        return remote(ref, ref, q_send.at[way, step], q_recv.at[way, step], device)
-
-    def y_units(way, step):
-        if 2 * step < ny:
-            return (0, 1, 2)
-        return (0, 2) if way == 0 else (1,)
-
-    def y_slot(way, step):
-        return lax.rem(y + ny - step, ny) if way == 0 else lax.rem(y + step, ny)
-
-    def z_slot(way, step):
-        return lax.rem(z + nz - step, nz) if way == 0 else lax.rem(z + step, nz)
+        target = on_b(shifted(b, 1 if way == 0 else -1))
+        return remote(ref, ref, q_send.at[way, step], q_recv.at[way, step], target)
+
+    def a_units(way, step):
+        if 2 * step < size:
+            return (0, 1)
+        return (0,) if way == 0 else (1,)
+
+    def slot_of(place, way, step):
+        return shifted(place, -step if way == 0 else step)
+
+    def b_ways(step):
+        return (0, 1) if 2 * step < size else (0,)
 
     started = []
 
@@ -276,18 +297,11 @@
         copy.start()
         started.append(copy)
 
-    def y_begin(step, units):
-        for unit in units:
-            for way in (0, 1):
-                if unit in y_units(way, step):
-                    begin(y_copy(way, unit, y_slot(way, step - 1), step - 1))
-
-    def z_ways(step):
-        return (0, 1) if 2 * step < nz else (0,)
-
-    y_begin(1, (0, 1))
-    for way in z_ways(1):
-        begin(z_copy(way, z, 0))
+    for unit in (0, 1):
+        for way in (0, 1):
+            begin(a_copy(way, unit, a, 0))
+    for way in (0, 1):
+        begin(b_copy(way, b, 0))
 
     queries = proj_ref[:, 0:128].astype(F32)
     forget = proj_ref[:, 128:256].astype(F32)
@@ -299,15 +313,31 @@
     cols_i = lax.broadcasted_iota(jnp.int32, (height, height), 1)
     lower = jnp.where(cols_i <= rows_i, 1.0, 0.0).astype(BF16)
     sums = jnp.zeros((height, 128), F32)
-    for part in thirds(decays):
-        sums = sums + jnp.dot(lower, part, preferred_element_type=F32)
+    for third in thirds(decays):
+        sums = sums + jnp.dot(lower, third, preferred_element_type=F32)
     ending = sums[height - 1 : height, :]
     kept = (inflow * jnp.exp(ending - sums)).astype(BF16)
     values_rt = jnp.transpose(values.astype(F32)).astype(BF16)
-    sbuf[y] = jnp.concatenate(
-        [jnp.dot(values_rt, kept, preferred_element_type=F32).astype(BF16), padded_thirds([ending], 16)], axis=0
-    )
-    y_begin(1, (2,))
+    own_state = jnp.dot(values_rt, kept, preferred_element_type=F32).astype(BF16)
+
+    part = 128 // size
+    logs = padded_thirds([ending], 16)
+    for target in range(size):
+        slice_out[target] = jnp.concatenate([own_state[target * part : (target + 1) * part], logs], axis=0)
+    slice_in[y] = slice_out[y]
+    turned = jnp.transpose(start_ref[...])
+    for slot in range(size):
+        start_t[slot] = turned[slot * part : (slot + 1) * part]
+
+    def slice_copy(source, target):
+        return remote(
+            slice_out.at[target], slice_in.at[source], s_send.at[target], s_recv.at[source], {"y": target}
+        )
+
+    @pl.loop(1, size)
+    def _(step):
+        slice_copy(y, shifted(y, step)).start()
+
     mixing = []
     for at in range(0, height, SUB):
         reach = 128 if at + SUB <= 128 else height
@@ -322,9 +352,9 @@
     local_out = jnp.dot(mixing.astype(BF16), values, preferred_element_type=F32)
     carried_query = (queries * jnp.exp(sums)).astype(BF16)
 
-    reference_gate = gates(z, ny - 1)[:, height - 1 : height]
-    for slot in range(ny):
-        relative = reference_gate - gates(z, slot)
+    reference_gate = key_gates(mine * (size - 1) + c * z)[:, height - 1 : height]
+    for slot in range(size):
+        relative = reference_gate - key_gates(slot)
         for head in range(2):
             bias[slot, head] = jnp.transpose(jnp.broadcast_to(relative[head : head + 1], (128, height)))
     top[...] = jnp.full(top.shape, LOW, F32)
@@ -332,46 +362,43 @@
     ones = jnp.ones((16, height), BF16)
     blank = jnp.zeros((FD, height), BF16)
 
-    def update(zq, yk, own):
-        keys = kbuf[yk]
+    def split_query(iq, head):
+        piece = qbuf[iq, head * FD : (head + 1) * FD]
+        return jnp.concatenate([piece, blank] if head == 0 else [blank, piece], axis=0)
+
+    def with_ones(ik, head):
+        return jnp.concatenate([vbuf[ik, head * FD : (head + 1) * FD], ones], axis=0)
+
+    def wide(column):
+        return jnp.concatenate([column] * (height // 128), axis=1)
+
+    def fold_own():
         for head in range(2):
-            part = qbuf[zq, head * FD : (head + 1) * FD]
-            split = jnp.concatenate([part, blank] if head == 0 else [blank, part], axis=0)
-            scores = jnp.dot(keys, split, preferred_element_type=F32)
-            shift = bias[yk, head]
-            scores = scores + jnp.concatenate([shift] * (height // 128), axis=1)
-            if own:
-                scores = jnp.where(rows_i <= cols_i, scores, LOW)
-            old = top[zq, head]
-            new = jnp.maximum(old, jnp.max(scores, axis=0, keepdims=True))
-            weights = jnp.exp(scores - new[0:1])
-            rescale = jnp.exp(old - new)[0:1]
-            top[zq, head] = new
-            left = jnp.concatenate([vbuf[yk, head * FD : (head + 1) * FD], ones], axis=0)
-            acc[zq, head] = acc[zq, head] * rescale + jnp.dot(
-                left, weights.astype(BF16), preferred_element_type=F32
-            )
-
-    update(z, y, True)
+            scores = jnp.dot(kbuf[a], split_query(b, head), preferred_element_type=F32) + wide(bias[a, head])
+            scores = jnp.where(rows_i <= cols_i, scores, LOW)
+            new = jnp.broadcast_to(jnp.max(scores, axis=0, keepdims=True), (8, height))
+            top[b, head] = new
+            weights = jnp.exp(scores - new[0:1]).astype(BF16)
+            acc[b, head] = jnp.dot(with_ones(a, head), weights, preferred_element_type=F32)
+
+    fold_own()
 
     def pipeline(count, place):
         def at(number):
             return place(jnp.clip(number, 0, count - 1))
 
         def scores_of(number, lane):
-            zq, yk = at(number)
-            keys = kbuf[yk]
-            later = jnp.where((zq == z) & (yk > y), LOW, 0.0)
+            iq, ik = at(number)
+            keys = kbuf[ik]
+            row, column = mine * iq + c * ik, mine * ik + c * iq
+            later = jnp.where((row == z) & ((column - y) * (mine - c) > 0), LOW, 0.0)
             for head in range(2):
-                part = qbuf[zq, head * FD : (head + 1) * FD]
-                split = jnp.concatenate([part, blank] if head == 0 else [blank, part], axis=0)
-                scores = jnp.dot(keys, split, preferred_element_type=F32)
-                shift = bias[yk, head] + later
-                scores = scores + jnp.concatenate([shift] * (height // 128), axis=1)
-                old = top[zq, head]
+                scores = jnp.dot(keys, split_query(iq, head), preferred_element_type=F32)
+                scores = scores + wide(bias[ik, head] + later)
+                old = top[iq, head]
                 new = jnp.maximum(old, jnp.max(scores, axis=0, keepdims=True))
                 score_s[lane, head] = scores
-                top[zq, head] = new
+                top[iq, head] = new
                 top_s[lane, head] = new
                 scale_s[lane, head] = jnp.exp(old - new)
 
@@ -381,11 +408,10 @@
                 scale_w[lane, head] = scale_s[lane, head]
 
         def sums_of(number, lane):
-            zq, yk = at(number)
+            iq, ik = at(number)
             for head in range(2):
-                left = jnp.concatenate([vbuf[yk, head * FD : (head + 1) * FD], ones], axis=0)
-                acc[zq, head] = acc[zq, head] * scale_w[lane, head][0:1] + jnp.dot(
-                    left, weight_s[lane, head], preferred_element_type=F32
+                acc[iq, head] = acc[iq, head] * scale_w[lane, head][0:1] + jnp.dot(
+                    with_ones(ik, head), weight_s[lane, head], preferred_element_type=F32
                 )
 
         weight_s[...] = jnp.zeros_like(weight_s)
@@ -410,102 +436,136 @@
             def _(number=number, lane=lane):
                 sums_of(number, lane)
 
+    reach = mine * (size - 1 - z) + c * z
+
     def fold(step):
-        last = 2 * step == nz
-        back = min(step, nz // 2 - 1)
-        ahead = jnp.minimum(step, nz - 1 - z) + 1
-        behind = jnp.maximum(back - z, 0)
+        last = 2 * step == size
+        back = min(step, size // 2 - 1)
+        ahead = jnp.minimum(step, reach) + 1
+        behind = jnp.maximum(back - (size - 1 - reach), 0)
         fresh = 1 if last else 2
         first = (ahead + behind) * fresh
-        one = jnp.where(z + step <= nz - 1, 1, 0)
-        two = 0 if last else jnp.where(z <= step - 1, 1, 0)
+        one = jnp.where(step <= reach, 1, 0)
+        two = 0 if last else jnp.where(size - step <= reach, 1, 0)
         known = 2 * step - 1
 
         def place(number):
             which = number // fresh
-            oq = jnp.where(which < ahead, which, nz - back + which - ahead)
-            ok = step if last else (number % 2) * (2 * step) - step
+            bounded = jnp.where(which < ahead, which, size - back + which - ahead)
+            free = step if last else (number % 2) * (2 * step) - step
             rest = jnp.maximum(number - first, 0)
-            second = rest // known
-            oq_new = jnp.where((second == 0) & (one == 1), step, nz - step)
-            ok_new = rest % known - (step - 1)
+            bounded_new = jnp.where((rest // known == 0) & (one == 1), step, size - step)
+            free_new = rest % known - (step - 1)
             old = number < first
-            return z + jnp.where(old, oq, oq_new), lax.rem(y + jnp.where(old, ok, ok_new) + ny, ny)
+            bounded, free = jnp.where(old, bounded, bounded_new), jnp.where(old, free, free_new)
+            iq = mine * (b + bounded) + c * shifted(b, free)
+            ik = mine * shifted(a, free) + c * (a - bounded)
+            return iq, ik
 
         pipeline(first + (one + two) * known, place)
 
-    for step in range(1, ny // 2 + 1):
-        for unit in (0, 1, 2):
+    def log_of(block):
+        return block[part : part + 1] + block[part + 1 : part + 2] + block[part + 2 : part + 3]
+
+    def total_copy(source, target):
+        ref = total_in.at[source]
+        return remote(ref, ref, t_send.at[target], t_recv.at[source], {"z": target})
+
+    def state_copy(source, target):
+        return remote(state_out.at[target], state_in.at[source], u_send.at[target], u_recv.at[source], {"y": target})
+
+    def row_states():
+        @pl.loop(1, size)
+        def _(step):
+            source = shifted(y, -step)
+            slice_copy(source, y).wait_recv()
+
+        state = jnp.zeros((part, 128), F32)
+        log_all = jnp.zeros((1, 128), F32)
+        for slot in range(size):
+            prefix[slot] = state
+            log_prefix[slot] = jnp.broadcast_to(log_all, (8, 128))
+            block = slice_in[slot].astype(F32)
+            log_own = log_of(block)
+            state = state * jnp.exp(log_own) + block[:part]
+            log_all = log_all + log_own
+        total_in[z] = jnp.concatenate([state.astype(BF16), padded_thirds([log_all], 16)], axis=0)
+
+        @pl.loop(z + 1, size)
+        def _(target):
+            total_copy(z, target).start()
+
+    def all_states():
+        def take(slot, state):
+            total_copy(slot, z).wait_recv()
+            block = total_in[slot].astype(F32)
+            return state * jnp.exp(log_of(block)) + block[:part]
+
+        incoming = lax.fori_loop(0, z, take, start_t[y])
+        for slot in range(size):
+            state = incoming * jnp.exp(log_prefix[slot][0:1]) + prefix[slot]
+            state_out[slot] = state.astype(BF16)
+        state_in[y] = state_out[y]
+
+        @pl.loop(1, size)
+        def _(step):
+            state_copy(y, shifted(y, step)).start()
+
+    for step in range(1, size // 2 + 1):
+        for unit in (0, 1):
             for way in (0, 1):
-                if unit in y_units(way, step):
-                    slot = y_slot(way, step)
-                    y_copy(way, unit, slot, step - 1).wait_recv()
-                    if unit in y_units(way, step + 1) and step < ny // 2:
-                        begin(y_copy(way, unit, slot, step))
-        for way in z_ways(step):
-            slot = z_slot(way, step)
-            z_copy(way, slot, step - 1).wait_recv()
-            if step < nz // 2 and way in z_ways(step + 1):
-                begin(z_copy(way, slot, step))
-        if step < ny // 2:
-            fold(step)
-        else:
-            state = jnp.zeros((128, 128), F32)
-            inside = state
-            log_all = jnp.zeros((1, 128), F32)
-            log_before = log_all
-            for slot in range(ny):
-                block = sbuf[slot].astype(F32)
-                log_own = block[128:129] + block[129:130] + block[130:131]
-                state = state * jnp.exp(log_own) + block[:128]
-                log_all = log_all + log_own
-                inside = jnp.where(slot < y, state, inside)
-                log_before = jnp.where(slot < y, log_all, log_before)
-            tbuf[z] = jnp.concatenate([state.astype(BF16), padded_thirds([log_all], 16)], axis=0)
-
-            def t_copy(slot, target):
-                ref = tbuf.at[slot]
-                return remote(ref, ref, t_send.at[target], t_recv.at[slot], {"z": target})
-
-            @pl.loop(z + 1, nz)
-            def _(target):
-                t_copy(z, target).start()
-
-            fold(step)
+                if unit in a_units(way, step):
+                    slot = slot_of(a, way, step)
+                    a_copy(way, unit, slot, step - 1).wait_recv()
+                    if 2 * step < size and unit in a_units(way, step + 1):
+                        begin(a_copy(way, unit, slot, step))
+        for way in b_ways(step):
+            slot = slot_of(b, way, step)
+            b_copy(way, slot, step - 1).wait_recv()
+            if 2 * step < size and way in b_ways(step + 1):
+                begin(b_copy(way, slot, step))
+        fold(step)
+        if step == 1:
+            row_states()
+        if step == 2:
+            all_states()
 
     def o_copy(source, slot, target):
-        return remote(obuf.at[slot], rbuf.at[source], o_send.at[slot], o_recv.at[source], {"z": target})
-
-    def logs_of(zq):
-        shift = gates(zq, y) - reference_gate
+        return remote(obuf.at[slot], rbuf.at[source], o_send.at[slot], o_recv.at[source], on_b(target))
+
+    def logs_of(iq):
+        shift = query_gates(iq) - reference_gate
         return [
-            top[zq, head][0:1] + jnp.log(acc[zq, head][FD : FD + 1]) + shift[head : head + 1] for head in range(2)
+            top[iq, head][0:1] + jnp.log(acc[iq, head][FD : FD + 1]) + shift[head : head + 1] for head in range(2)
         ]
 
-    def rows_of(zq):
-        return [acc[zq, head][:FD] / acc[zq, head][FD : FD + 1] for head in range(2)]
-
-    @pl.loop(z + 1, nz)
-    def _(target):
+    def rows_of(iq):
+        return [acc[iq, head][:FD] / acc[iq, head][FD : FD + 1] for head in range(2)]
+
+    sent = mine * (size - 1 - z) + c * (size - 1)
+    received = mine * z + c * (size - 1)
+
+    @pl.loop(1, sent + 1)
+    def _(step):
+        target = shifted(b, step)
         obuf[target] = jnp.concatenate(
-            [part.astype(BF16) for part in rows_of(target)] + [padded_thirds(logs_of(target), 16)], axis=0
+            [piece.astype(BF16) for piece in rows_of(target)] + [padded_thirds(logs_of(target), 16)], axis=0
         )
-        o_copy(z, target, target).start()
-
-    def take(slot, state):
-        t_copy(slot, z).wait_recv()
-        block = tbuf[slot].astype(F32)
-        log_own = block[128:129] + block[129:130] + block[130:131]
-        return state * jnp.exp(log_own) + block[:128]
-
-    arriving = lax.fori_loop(0, z, take, jnp.transpose(start_ref[...]))
-    arriving = arriving * jnp.exp(log_before) + inside
-    rec_out = local_out + nt(carried_query, arriving.astype(BF16))
+        o_copy(b, target, target).start()
+
+    @pl.loop(1, size)
+    def _(step):
+        source = shifted(y, -step)
+        state_copy(source, y).wait_recv()
+
+    arriving = jnp.concatenate([state_in[slot] for slot in range(size)], axis=0)
+    rec_out = local_out + nt(carried_query, arriving)
     mean = jnp.mean(rec_out * rec_out, axis=1, keepdims=True)
     out_ref[:, 0:128] = (rec_out * lax.rsqrt(mean + EPSILON) * recur_gain_ref[...]).astype(BF16)
 
-    def merge(slot, carry):
-        o_copy(slot, slot, z).wait_recv()
+    def merge(step, carry):
+        slot = shifted(b, -step)
+        o_copy(slot, slot, b).wait_recv()
         block = rbuf[slot].astype(F32)
         merged = []
         for head in range(2):
@@ -517,11 +577,11 @@
             merged += [new, amount * keep + add, rows * keep + block[head * FD : (head + 1) * FD] * add]
         return tuple(merged)
 
-    own_logs, own_rows = logs_of(z), rows_of(z)
+    own_logs, own_rows = logs_of(b), rows_of(b)
     start = []
     for head in range(2):
         start += [own_logs[head], jnp.ones((1, height), F32), own_rows[head]]
-    merged = lax.fori_loop(0, z, merge, tuple(start))
+    merged = lax.fori_loop(1, received + 1, merge, tuple(start))
     normed = []
     for head in range(2):
         rows = merged[3 * head + 2] / merged[3 * head + 1]
@@ -533,10 +593,19 @@
     for copy in started:
         copy.wait_send()
 
-    @pl.loop(z + 1, nz)
+    @pl.loop(1, size)
+    def _(step):
+        slice_copy(y, shifted(y, step)).wait_send()
+        state_copy(y, shifted(y, step)).wait_send()
+
+    @pl.loop(z + 1, size)
     def _(target):
-        t_copy(z, target).wait_send()
-        o_copy(z, target, target).wait_send()
+        total_copy(z, target).wait_send()
+
+    @pl.loop(1, sent + 1)
+    def _(step):
+        target = shifted(b, step)
+        o_copy(b, target, target).wait_send()
 
 
 VM = pl.BlockSpec(memory_space=pltpu.VMEM)
@@ -572,38 +641,42 @@
     )(tokens, norm_gain.reshape(2 * nx, 1, features), *weights)
 
 
-def middle(nz, ny, projected, gate_floor, extra_decay, start_state, recur_gain, gate_cache, attend_gain):
+def middle(size, projected, gate_floor, extra_decay, start_state, recur_gain, gate_cache, attend_gain):
     height = projected.shape[0]
+    part = 128 // size
     return pl.pallas_call(
-        functools.partial(middle_kernel, nz, ny),
+        functools.partial(middle_kernel, size),
         out_shape=jax.ShapeDtypeStruct((height, 256), BF16),
         in_specs=[VM] * 7,
         out_specs=VM,
         scratch_shapes=[
-            pltpu.VMEM((ny, height, 128), BF16),
-            pltpu.VMEM((ny, 128, height), BF16),
-            pltpu.VMEM((nz, 128, height), BF16),
-            pltpu.VMEM((ny, 144, 128), BF16),
-            pltpu.VMEM((nz, 144, 128), BF16),
-            pltpu.VMEM((nz, 144, height), BF16),
-            pltpu.VMEM((nz, 144, height), BF16),
-            pltpu.VMEM((nz, 2, FD + 16, height), F32),
-            pltpu.VMEM((nz, 2, 8, height), F32),
-            pltpu.VMEM((ny, 2, height, 128), F32),
+            pltpu.VMEM((size, height, 128), BF16),
+            pltpu.VMEM((size, 128, height), BF16),
+            pltpu.VMEM((size, 128, height), BF16),
+            pltpu.VMEM((size, part + 16, 128), BF16),
+            pltpu.VMEM((size, part + 16, 128), BF16),
+            pltpu.VMEM((size, part + 16, 128), BF16),
+            pltpu.VMEM((size, part, 128), BF16),
+            pltpu.VMEM((size, part, 128), BF16),
+            pltpu.VMEM((size, part, 128), F32),
+            pltpu.VMEM((size, part, 128), F32),
+            pltpu.VMEM((size, 8, 128), F32),
+            pltpu.VMEM((size, 144, height), BF16),
+            pltpu.VMEM((size, 144, height), BF16),
+            pltpu.VMEM((size, 2, FD + 16, height), F32),
+            pltpu.VMEM((size, 2, 8, height), F32),
+            pltpu.VMEM((size, 2, height, 128), F32),
             pltpu.VMEM((LANES, 2, height, height), F32),
             pltpu.VMEM((LANES, 2, height, height), BF16),
             pltpu.VMEM((LANES, 2, 8, height), F32),
             pltpu.VMEM((LANES, 2, 8, height), F32),
             pltpu.VMEM((LANES, 2, 8, height), F32),
-            DMA((2, 3, ny // 2)),
-            DMA((2, 3, ny // 2)),
-            DMA((2, nz // 2)),
-            DMA((2, nz // 2)),
-            DMA((nz,)),
-            DMA((nz,)),
-            DMA((nz,)),
-            DMA((nz,)),
-        ],
+            DMA((2, 2, size // 2)),
+            DMA((2, 2, size // 2)),
+            DMA((2, size // 2)),
+            DMA((2, size // 2)),
+        ]
+        + [DMA((size,))] * 8,
         compiler_params=params(1),
         name="middle",
     )(
@@ -658,10 +731,10 @@
     recur_output,
     attend_output,
 ):
-    nz, ny, nx = sizes
+    _, ny, nx = sizes
     weights = (recur_query, recur_forget, recur_value, attend_query, attend_key, attend_value)
     projected = project(nx, tokens, norm_gain, weights)
-    rows = middle(nz, ny, projected, gate_floor, extra_decay, start_state, recur_gain, gate_cache, attend_gain)
+    rows = middle(ny, projected, gate_floor, extra_decay, start_state, recur_gain, gate_cache, attend_gain)
     return output(nx, rows, recur_output, attend_output)
 
 

time: 81.9 us -> 73.5 us (0.90)
  Pallas kernels: 80 us -> 71.6 us
    pallas_call x1, Pallas kernels: 48.6 us -> 38.2 us  [middle(): pl.pallas_call(functools.partial(middle_kernel, size), out_shape=jax.Shap...]
    pallas_call x1, Pallas kernels: 12.5 us -> 14.5 us  [output(): pl.pallas_call(functools.partial(output_kernel, nx), out_shape=jax.ShapeD...]
where the time goes in v3:
time: 73.5 us; the launch traced here: 73.2 us
  Pallas kernels  71.6 us (97%)
  local copies, waits for them, and re-layouts  1.57 us (2%)
    pallas_call x1, Pallas kernels, middle(): pl.pallas_call(functools.partial(middle_kernel, size), out_shape=jax.Shap...  38.2 us
    pallas_call x1, Pallas kernels, project(): pl.pallas_call(functools.partial(project_kernel, nx), out_shape=jax.Shape...  18.9 us
    pallas_call x1, Pallas kernels, output(): pl.pallas_call(functools.partial(output_kernel, nx), out_shape=jax.ShapeD...  14.5 us
    unnamed x1, local copies, waits for them, and re-layouts  1.57 us

profile of v3, /device:TPU:1, one launch (start us, length us, event | category | flops | bytes accessed | tf_op | source)
XLA Modules:
  0.0 73.2 jit_solution(896990031922607553)
XLA Ops:
  0.0 18.9 %project.1.proj_ref = bf16[256,768]{1,0:T(8,128)(2,1)} custom-call(bf16[256,256]{1,0:T(8,128)(2,1)} %tokens_ref.1, f32[8,1,256]{2,1,0:T(1,128)} %bitcast.9, bf16[2048,128]{1,0:T(8,128)(2,1)} %refs_0_.1, bf16[2048,128]{1,0:T(8,128)(2,1)} %refs_1_.1, bf16[2048,128]{1,0:T(8,128)(2,1)} %refs_2_.1, bf16[2048,128]{1,0:T(8,128)(2,1)} %refs_3_.1, ...), custom_call_target="tpu_custom_call" | custom-call | tf_op jit(solution)/shard_map/project/pallas_call | solution.py:624
  18.9 38.2 %middle.1.rows_ref = bf16[256,256]{1,0:T(8,128)(2,1)} custom-call(bf16[256,768]{1,0:T(8,128)(2,1)} %project.1.proj_ref, f32[1,128]{1,0:T(1,128)} %bitcast.11, f32[1,256]{1,0:T(1,128)} %bitcast.10, f32[128,128]{1,0:T(8,128)} %bitcast.8, f32[1,128]{1,0:T(1,128)} %bitcast.12, f32[2,16384]{1,0:T(2,128)} %bitcast.7, f32[1,128]{1,0:T(1,128)} %bitcast.13), custom_call_target="tpu_custom_call" | custom-call | tf_op jit(solution)/shard_map/middle/pallas_call | solution.py:647
  57.2 14.5 %output.1 = bf16[256,256]{1,0:T(8,128)(2,1)} custom-call(bf16[256,256]{1,0:T(8,128)(2,1)} %middle.1.rows_ref, bf16[1024,256]{1,0:T(8,128)(2,1)} %recur_ref.1, bf16[1024,256]{1,0:T(8,128)(2,1)} %attend_ref.1), custom_call_target="tpu_custom_call" | custom-call | tf_op jit(solution)/shard_map/output/pallas_call | solution.py:696
  71.7 1.6 %copy.18 = bf16[256,256]{1,0:T(8,128)(2,1)} copy(bf16[256,256]{1,0:T(8,128)(2,1)} %output.1) | data formatting | bytes 262144

commit v4 on v3

--- a/solution.py
+++ b/solution.py
@@ -27,16 +27,7 @@
     )
 
 
-def tp_greet(nx):
-    x, c = lax.axis_index("x"), lax.axis_index("c")
-    barrier = pltpu.get_barrier_semaphore()
-    peers = [{"c": 1 - c}, {"x": lax.rem(x + 1, nx)}, {"x": lax.rem(x + nx - 1, nx)}]
-    for peer in peers:
-        pl.semaphore_signal(barrier, inc=1, device_id=peer, device_id_type=MESH)
-    pl.semaphore_wait(barrier, len(peers))
-
-
-def tp_gather(nx, slots, send_sem, recv_sem, consume):
+def tp_gather(nx, slots, send_sem, recv_sem, consume, pause=lambda: None):
     x, c = lax.axis_index("x"), lax.axis_index("c")
     other = 1 - c
     right, left, far = lax.rem(x + 1, nx), lax.rem(x + nx - 1, nx), lax.rem(x + 2, nx)
@@ -70,17 +61,20 @@
     forward(5, from_left, top, to_right)
     piece(1, from_right, bottom, to_left).wait_recv()
     forward(6, from_right, bottom, to_left)
+    pause()
     piece(4, 2 * x + other, None, to_other).wait_recv()
     consume(2 * x + other)
     piece(2, from_left, bottom, to_right).wait_recv()
     forward(7, from_left, None, to_other)
     piece(3, from_right, top, to_left).wait_recv()
     forward(8, from_right, None, to_other)
+    pause()
     consume(from_left)
     consume(from_right)
     piece(5, across, top, to_right).wait_recv()
     piece(6, across, bottom, to_left).wait_recv()
     forward(9, across, None, to_other)
+    pause()
     piece(7, 2 * left + other, None, to_other).wait_recv()
     consume(2 * left + other)
     piece(8, 2 * right + other, None, to_other).wait_recv()
@@ -92,81 +86,6 @@
         copy.wait_send()
 
 
-def project_kernel(
-    nx, tokens_ref, gain_ref, *refs
-):
-    weights, out_ref = refs[:6], refs[6]
-    slots, held, total, squares, local_sem, weight_sem, send_sem, recv_sem = refs[7:]
-    x, c = lax.axis_index("x"), lax.axis_index("c")
-    own = pltpu.make_async_copy(tokens_ref, slots.at[2 * x + c], local_sem)
-    own.start()
-    width = weights[0].shape[1]
-    loads = [
-        pltpu.make_async_copy(ref, held.at[:, pl.ds(n * width, width)], weight_sem.at[n])
-        for n, ref in enumerate(weights)
-    ]
-    for load in loads:
-        load.start()
-    total[...] = jnp.zeros_like(total)
-    squares[...] = jnp.zeros_like(squares)
-    tp_greet(nx)
-    own.wait()
-    features = tokens_ref.shape[1]
-    waited = []
-
-    def consume(p):
-        if not waited:
-            for load in loads:
-                load.wait()
-            waited.append(True)
-        wide = slots[p].astype(F32)
-        squared = wide * wide
-        folded = squared[:, :128]
-        for k in range(1, features // 128):
-            folded = folded + squared[:, k * 128 : (k + 1) * 128]
-        squares[...] += folded
-        scaled = (wide * gain_ref[p]).astype(BF16)
-        rows = pl.ds(pl.multiple_of(p * features, features), features)
-        total[...] += jnp.dot(scaled, held[rows, :], preferred_element_type=F32)
-
-    tp_gather(nx, slots, send_sem, recv_sem, consume)
-    mean = jnp.sum(squares[...], axis=1, keepdims=True) / held.shape[0]
-    inverse = lax.rsqrt(mean + EPSILON)
-    out_ref[...] = (total[...] * inverse).astype(BF16)
-
-
-def output_kernel(nx, rows_ref, recur_ref, attend_ref, out_ref, slots, held, total, local_sem, weight_sem, send_sem, recv_sem):
-    x, c = lax.axis_index("x"), lax.axis_index("c")
-    own = pltpu.make_async_copy(rows_ref, slots.at[2 * x + c], local_sem)
-    own.start()
-    depth = rows_ref.shape[1] // 2
-    pieces = 2 * nx
-    loads = []
-    for n in range(pieces):
-        for k, ref in enumerate((recur_ref, attend_ref)):
-            loads.append(
-                pltpu.make_async_copy(
-                    ref.at[pl.ds(n * depth, depth)], held.at[n, pl.ds(k * depth, depth)], weight_sem.at[2 * n + k]
-                )
-            )
-    for load in loads:
-        load.start()
-    total[...] = jnp.zeros_like(total)
-    tp_greet(nx)
-    own.wait()
-    waited = []
-
-    def consume(p):
-        if not waited:
-            for load in loads:
-                load.wait()
-            waited.append(True)
-        total[...] += jnp.dot(slots[p], held[p], preferred_element_type=F32)
-
-    tp_gather(nx, slots, send_sem, recv_sem, consume)
-    out_ref[...] = total[...].astype(BF16)
-
-
 def thirds(value):
     first = value.astype(BF16)
     rest = value - first.astype(F32)
@@ -189,16 +108,35 @@
     return lax.dot_general(left, right, (((1,), (1,)), ((), ())), preferred_element_type=F32)
 
 
-def middle_kernel(
+def layer_kernel(
     size,
-    proj_ref,
+    nx,
+    tokens_ref,
+    gain_ref,
+    weight_refs,
     floor_ref,
     decay_ref,
     start_ref,
     recur_gain_ref,
     gate_ref,
     attend_gain_ref,
+    recur_output_ref,
+    attend_output_ref,
     out_ref,
+    slots,
+    held,
+    total,
+    squares,
+    rows_slots,
+    held_out,
+    local_sem,
+    weight_sem,
+    output_sem,
+    token_send,
+    token_recv,
+    rows_send,
+    rows_recv,
+    chain,
     kbuf,
     vbuf,
     qbuf,
@@ -233,8 +171,47 @@
     o_send,
     o_recv,
 ):
-    z, y, c = lax.axis_index("z"), lax.axis_index("y"), lax.axis_index("c")
-    height = proj_ref.shape[0]
+    z, y, x, c = (lax.axis_index(name) for name in ("z", "y", "x", "c"))
+    height, features = tokens_ref.shape
+    me = 2 * x + c
+
+    def shifted(place, offset):
+        return lax.rem(place + offset + size, size)
+
+    own = pltpu.make_async_copy(tokens_ref, slots.at[me], local_sem)
+    own.start()
+    width = weight_refs[0].shape[1]
+    loads = [
+        pltpu.make_async_copy(ref, held.at[:, pl.ds(n * width, width)], weight_sem.at[n])
+        for n, ref in enumerate(weight_refs)
+    ]
+    depth = recur_output_ref.shape[0] // (2 * nx)
+    output_loads = [
+        pltpu.make_async_copy(
+            ref.at[pl.ds(n * depth, depth)], held_out.at[n, pl.ds(k * depth, depth)], output_sem.at[2 * n + k]
+        )
+        for n in range(2 * nx)
+        for k, ref in enumerate((recur_output_ref, attend_output_ref))
+    ]
+    for load in loads + output_loads:
+        load.start()
+
+    barrier = pltpu.get_barrier_semaphore()
+    along = [{"y": shifted(y, 1)}, {"y": shifted(y, -1)}, {"z": shifted(z, 1)}, {"z": shifted(z, -1)}]
+    for device in along + [{"c": 1 - c}, {"x": lax.rem(x + 1, nx)}, {"x": lax.rem(x + nx - 1, nx)}]:
+        pl.semaphore_signal(barrier, inc=1, device_id=device, device_id_type=MESH)
+
+    def pass_on():
+        for number, device in enumerate(along):
+            pl.semaphore_signal(chain.at[number], inc=1, device_id=device, device_id_type=MESH)
+
+    def hear():
+        for number in range(4):
+            pl.semaphore_wait(chain.at[number], 1)
+
+    total[...] = jnp.zeros_like(total)
+    squares[...] = jnp.zeros_like(squares)
+
     mine = 1 - c
     a, b = mine * y + c * z, mine * z + c * y
 
@@ -253,20 +230,45 @@
     def query_gates(index):
         return gates(mine * (index * size + y) + c * (z * size + index))
 
-    def shifted(place, offset):
-        return lax.rem(place + offset + size, size)
-
-    barrier = pltpu.get_barrier_semaphore()
-    for step in range(1, size):
-        for device in ({"y": shifted(y, step)}, {"z": shifted(z, step)}):
-            pl.semaphore_signal(barrier, inc=1, device_id=device, device_id_type=MESH)
-
-    kbuf[a] = proj_ref[:, 512:640]
-    values_t = jnp.transpose(proj_ref[:, 640:768].astype(F32))
-    vbuf[a] = values_t.astype(BF16)
-    query_t = jnp.transpose(proj_ref[:, 384:512].astype(F32) * (FD**-0.5))
-    qbuf[b] = query_t.astype(BF16)
-    pl.semaphore_wait(barrier, 2 * (size - 1))
+    reference_gate = key_gates(mine * (size - 1) + c * z)[:, height - 1 : height]
+    for slot in range(size):
+        relative = reference_gate - key_gates(slot)
+        for head in range(2):
+            bias[slot, head] = jnp.transpose(jnp.broadcast_to(relative[head : head + 1], (128, height)))
+    top[...] = jnp.full(top.shape, LOW, F32)
+    acc[...] = jnp.zeros_like(acc)
+    pl.semaphore_wait(barrier, 7)
+    pass_on()
+    own.wait()
+    waited = []
+    rounds_left = [True, True, False]
+
+    def pause():
+        hear()
+        if rounds_left.pop(0):
+            pass_on()
+
+    def consume(p):
+        if not waited:
+            for load in loads:
+                load.wait()
+            waited.append(True)
+        tokens = slots[p].astype(F32)
+        squared = tokens * tokens
+        folded = squared[:, :128]
+        for k in range(1, features // 128):
+            folded = folded + squared[:, k * 128 : (k + 1) * 128]
+        squares[...] += folded
+        scaled = (tokens * gain_ref[p]).astype(BF16)
+        rows = pl.ds(pl.multiple_of(p * features, features), features)
+        total[...] += jnp.dot(scaled, held[rows, :], preferred_element_type=F32)
+
+    tp_gather(nx, slots, token_send, token_recv, consume, pause)
+    mean = jnp.sum(squares[...], axis=1, keepdims=True) / held.shape[0]
+    inverse = lax.rsqrt(mean + EPSILON)
+
+    def projected(number):
+        return (total[:, number * 128 : (number + 1) * 128] * inverse).astype(BF16)
 
     kv = (kbuf, vbuf)
 
@@ -297,15 +299,19 @@
         copy.start()
         started.append(copy)
 
-    for unit in (0, 1):
-        for way in (0, 1):
-            begin(a_copy(way, unit, a, 0))
+    kbuf[a] = projected(4)
+    for way in (0, 1):
+        begin(a_copy(way, 0, a, 0))
+    vbuf[a] = jnp.transpose(projected(5).astype(F32)).astype(BF16)
+    for way in (0, 1):
+        begin(a_copy(way, 1, a, 0))
+    qbuf[b] = jnp.transpose(projected(3).astype(F32) * (FD**-0.5)).astype(BF16)
     for way in (0, 1):
         begin(b_copy(way, b, 0))
 
-    queries = proj_ref[:, 0:128].astype(F32)
-    forget = proj_ref[:, 128:256].astype(F32)
-    values = proj_ref[:, 256:384]
+    queries = projected(0).astype(F32)
+    forget = projected(1).astype(F32)
+    values = projected(2)
     inflow = (1.0 - floor_ref[...]) / (1.0 + jnp.exp(forget))
     extra = jnp.transpose(jnp.broadcast_to(decay_ref[...], (128, height)))
     decays = jnp.log1p(-inflow) - extra
@@ -352,13 +358,6 @@
     local_out = jnp.dot(mixing.astype(BF16), values, preferred_element_type=F32)
     carried_query = (queries * jnp.exp(sums)).astype(BF16)
 
-    reference_gate = key_gates(mine * (size - 1) + c * z)[:, height - 1 : height]
-    for slot in range(size):
-        relative = reference_gate - key_gates(slot)
-        for head in range(2):
-            bias[slot, head] = jnp.transpose(jnp.broadcast_to(relative[head : head + 1], (128, height)))
-    top[...] = jnp.full(top.shape, LOW, F32)
-    acc[...] = jnp.zeros_like(acc)
     ones = jnp.ones((16, height), BF16)
     blank = jnp.zeros((FD, height), BF16)
 
@@ -561,7 +560,7 @@
     arriving = jnp.concatenate([state_in[slot] for slot in range(size)], axis=0)
     rec_out = local_out + nt(carried_query, arriving)
     mean = jnp.mean(rec_out * rec_out, axis=1, keepdims=True)
-    out_ref[:, 0:128] = (rec_out * lax.rsqrt(mean + EPSILON) * recur_gain_ref[...]).astype(BF16)
+    rows_slots[me, :, 0:128] = (rec_out * lax.rsqrt(mean + EPSILON) * recur_gain_ref[...]).astype(BF16)
 
     def merge(step, carry):
         slot = shifted(b, -step)
@@ -588,7 +587,18 @@
         mean = jnp.mean(rows * rows, axis=0, keepdims=True)
         normed.append(rows * lax.rsqrt(mean + EPSILON))
     att_rows = jnp.transpose(jnp.concatenate(normed, axis=0))
-    out_ref[:, 128:256] = (att_rows * attend_gain_ref[...]).astype(BF16)
+    rows_slots[me, :, 128:256] = (att_rows * attend_gain_ref[...]).astype(BF16)
+
+    total_out = total.at[:, pl.ds(0, out_ref.shape[1])]
+    total_out[...] = jnp.zeros(out_ref.shape, F32)
+    for load in output_loads:
+        load.wait()
+
+    def consume_rows(p):
+        total_out[...] += jnp.dot(rows_slots[p], held_out[p], preferred_element_type=F32)
+
+    tp_gather(nx, rows_slots, rows_send, rows_recv, consume_rows)
+    out_ref[...] = total_out[...].astype(BF16)
 
     for copy in started:
         copy.wait_send()
@@ -617,39 +627,36 @@
     return pltpu.CompilerParams(collective_id=number, has_side_effects=True, vmem_limit_bytes=VMEM_LIMIT)
 
 
-def project(nx, tokens, norm_gain, weights):
+def unpack(size, nx, *refs):
+    layer_kernel(size, nx, refs[0], refs[1], refs[2:8], *refs[8:])
+
+
+def layer(size, nx, tokens, norm_gain, weights, gate_floor, extra_decay, start_state, recur_gain, gate_cache, attend_gain, recur_output, attend_output):
     height, features = tokens.shape
     model = norm_gain.shape[0]
     width = sum(weight.shape[1] for weight in weights)
+    out_width = recur_output.shape[1]
+    part = 128 // size
     return pl.pallas_call(
-        functools.partial(project_kernel, nx),
-        out_shape=jax.ShapeDtypeStruct((height, width), BF16),
-        in_specs=[ANY, VM] + [ANY] * 6,
+        functools.partial(unpack, size, nx),
+        out_shape=jax.ShapeDtypeStruct((height, out_width), BF16),
+        in_specs=[ANY, VM] + [ANY] * 6 + [VM] * 6 + [ANY] * 2,
         out_specs=VM,
         scratch_shapes=[
             pltpu.VMEM((2 * nx, height, features), BF16),
             pltpu.VMEM((model, width), BF16),
             pltpu.VMEM((height, width), F32),
             pltpu.VMEM((height, 128), F32),
+            pltpu.VMEM((2 * nx, height, 256), BF16),
+            pltpu.VMEM((2 * nx, 256, out_width), BF16),
             DMA,
             DMA((6,)),
+            DMA((4 * nx,)),
             DMA((10,)),
             DMA((10,)),
-        ],
-        compiler_params=params(0),
-        name="project",
-    )(tokens, norm_gain.reshape(2 * nx, 1, features), *weights)
-
-
-def middle(size, projected, gate_floor, extra_decay, start_state, recur_gain, gate_cache, attend_gain):
-    height = projected.shape[0]
-    part = 128 // size
-    return pl.pallas_call(
-        functools.partial(middle_kernel, size),
-        out_shape=jax.ShapeDtypeStruct((height, 256), BF16),
-        in_specs=[VM] * 7,
-        out_specs=VM,
-        scratch_shapes=[
+            DMA((10,)),
+            DMA((10,)),
+            pltpu.SemaphoreType.REGULAR((4,)),
             pltpu.VMEM((size, height, 128), BF16),
             pltpu.VMEM((size, 128, height), BF16),
             pltpu.VMEM((size, 128, height), BF16),
@@ -677,39 +684,21 @@
             DMA((2, size // 2)),
         ]
         + [DMA((size,))] * 8,
-        compiler_params=params(1),
-        name="middle",
+        compiler_params=params(0),
+        name="layer",
     )(
-        projected,
+        tokens,
+        norm_gain.reshape(2 * nx, 1, features),
+        *weights,
         gate_floor.reshape(1, -1),
         extra_decay.reshape(1, -1),
         start_state.reshape(128, 128),
         recur_gain.reshape(1, -1),
         gate_cache.T,
         attend_gain.reshape(1, -1),
+        recur_output,
+        attend_output,
     )
-
-
-def output(nx, rows, recur_output, attend_output):
-    height = rows.shape[0]
-    width = recur_output.shape[1]
-    return pl.pallas_call(
-        functools.partial(output_kernel, nx),
-        out_shape=jax.ShapeDtypeStruct((height, width), BF16),
-        in_specs=[ANY] * 3,
-        out_specs=VM,
-        scratch_shapes=[
-            pltpu.VMEM((2 * nx, height, 256), BF16),
-            pltpu.VMEM((2 * nx, 256, width), BF16),
-            pltpu.VMEM((height, width), F32),
-            DMA,
-            DMA((4 * nx,)),
-            DMA((10,)),
-            DMA((10,)),
-        ],
-        compiler_params=params(2),
-        name="output",
-    )(rows, recur_output, attend_output)
 
 
 def shards(
@@ -733,9 +722,7 @@
 ):
     _, ny, nx = sizes
     weights = (recur_query, recur_forget, recur_value, attend_query, attend_key, attend_value)
-    projected = project(nx, tokens, norm_gain, weights)
-    rows = middle(ny, projected, gate_floor, extra_decay, start_state, recur_gain, gate_cache, attend_gain)
-    return output(nx, rows, recur_output, attend_output)
+    return layer(ny, nx, tokens, norm_gain, weights, gate_floor, extra_decay, start_state, recur_gain, gate_cache, attend_gain, recur_output, attend_output)
 
 
 def solution(mesh):

time: 73.5 us -> 63.8 us (0.87)
  Pallas kernels: 71.6 us -> 62.1 us
    pallas_call x3 -> x1, Pallas kernels: 71.6 us -> 62.1 us  [layer(): pl.pallas_call(functools.partial(unpack, size, nx), out_shape=jax.ShapeDt...]
where the time goes in v4:
time: 63.8 us; the launch traced here: 63.7 us
  Pallas kernels  62.1 us (97%)
  local copies, waits for them, and re-layouts  1.57 us (2%)
    pallas_call x1, Pallas kernels, layer(): pl.pallas_call(functools.partial(unpack, size, nx), out_shape=jax.ShapeDt...  62.1 us
    unnamed x1, local copies, waits for them, and re-layouts  1.57 us

profile of v4, /device:TPU:1, one launch (start us, length us, event | category | flops | bytes accessed | tf_op | source)
XLA Modules:
  0.0 63.7 jit_solution(7012184614295570726)
XLA Ops:
  0.0 62.1 %layer.1 = bf16[256,256]{1,0:T(8,128)(2,1)} custom-call(bf16[256,256]{1,0:T(8,128)(2,1)} %refs_0_.1, f32[8,1,256]{2,1,0:T(1,128)} %bitcast.9, bf16[2048,128]{1,0:T(8,128)(2,1)} %refs_2_.1, bf16[2048,128]{1,0:T(8,128)(2,1)} %refs_3_.1, bf16[2048,128]{1,0:T(8,128)(2,1)} %refs_4_.1, bf16[2048,128]{1,0:T(8,128)(2,1)} %refs_5_.1, bf16[2048,128]{1,0:T(8,128)(2,1)} %refs_6_.1, ...), custom_call_target="tpu_custom_call" | custom-call | tf_op jit(solution)/shard_map/layer/pallas_call | solution.py:640
  62.1 1.6 %copy.18 = bf16[256,256]{1,0:T(8,128)(2,1)} copy(bf16[256,256]{1,0:T(8,128)(2,1)} %layer.1) | data formatting | bytes 262144

commit v5 on v4

--- a/solution.py
+++ b/solution.py
@@ -27,7 +27,7 @@
     )
 
 
-def tp_gather(nx, slots, send_sem, recv_sem, consume, pause=lambda: None):
+def tp_gather(nx, slots, send_sem, recv_sem, consume, begun=lambda: None, pause=lambda: None):
     x, c = lax.axis_index("x"), lax.axis_index("c")
     other = 1 - c
     right, left, far = lax.rem(x + 1, nx), lax.rem(x + nx - 1, nx), lax.rem(x + 2, nx)
@@ -50,6 +50,7 @@
     ]
     for copy in sends:
         copy.start()
+    begun()
     consume(me)
 
     def forward(number, p, rows, device):
@@ -112,14 +113,14 @@
     size,
     nx,
     tokens_ref,
-    gain_ref,
+    gain_any,
     weight_refs,
-    floor_ref,
-    decay_ref,
-    start_ref,
-    recur_gain_ref,
-    gate_ref,
-    attend_gain_ref,
+    floor_any,
+    decay_any,
+    start_any,
+    recur_gain_any,
+    gate_any,
+    attend_gain_any,
     recur_output_ref,
     attend_output_ref,
     out_ref,
@@ -129,6 +130,14 @@
     squares,
     rows_slots,
     held_out,
+    gain_ref,
+    floor_ref,
+    decay_ref,
+    start_ref,
+    recur_gain_ref,
+    gate_ref,
+    attend_gain_ref,
+    small_sem,
     local_sem,
     weight_sem,
     output_sem,
@@ -178,6 +187,11 @@
     def shifted(place, offset):
         return lax.rem(place + offset + size, size)
 
+    barrier = pltpu.get_barrier_semaphore()
+    along = [{"y": shifted(y, 1)}, {"y": shifted(y, -1)}, {"z": shifted(z, 1)}, {"z": shifted(z, -1)}]
+    for device in along + [{"c": 1 - c}, {"x": lax.rem(x + 1, nx)}, {"x": lax.rem(x + nx - 1, nx)}]:
+        pl.semaphore_signal(barrier, inc=1, device_id=device, device_id_type=MESH)
+
     own = pltpu.make_async_copy(tokens_ref, slots.at[me], local_sem)
     own.start()
     width = weight_refs[0].shape[1]
@@ -193,13 +207,25 @@
         for n in range(2 * nx)
         for k, ref in enumerate((recur_output_ref, attend_output_ref))
     ]
-    for load in loads + output_loads:
+    for load in loads:
         load.start()
 
-    barrier = pltpu.get_barrier_semaphore()
-    along = [{"y": shifted(y, 1)}, {"y": shifted(y, -1)}, {"z": shifted(z, 1)}, {"z": shifted(z, -1)}]
-    for device in along + [{"c": 1 - c}, {"x": lax.rem(x + 1, nx)}, {"x": lax.rem(x + nx - 1, nx)}]:
-        pl.semaphore_signal(barrier, inc=1, device_id=device, device_id_type=MESH)
+    small_loads = [
+        pltpu.make_async_copy(source, target, small_sem.at[n])
+        for n, (source, target) in enumerate(
+            (
+                (gain_any, gain_ref),
+                (floor_any, floor_ref),
+                (decay_any, decay_ref),
+                (start_any, start_ref),
+                (recur_gain_any, recur_gain_ref),
+                (gate_any, gate_ref),
+                (attend_gain_any, attend_gain_ref),
+            )
+        )
+    ]
+    for load in small_loads + output_loads:
+        load.start()
 
     def pass_on():
         for number, device in enumerate(along):
@@ -230,13 +256,6 @@
     def query_gates(index):
         return gates(mine * (index * size + y) + c * (z * size + index))
 
-    reference_gate = key_gates(mine * (size - 1) + c * z)[:, height - 1 : height]
-    for slot in range(size):
-        relative = reference_gate - key_gates(slot)
-        for head in range(2):
-            bias[slot, head] = jnp.transpose(jnp.broadcast_to(relative[head : head + 1], (128, height)))
-    top[...] = jnp.full(top.shape, LOW, F32)
-    acc[...] = jnp.zeros_like(acc)
     pl.semaphore_wait(barrier, 7)
     pass_on()
     own.wait()
@@ -263,7 +282,19 @@
         rows = pl.ds(pl.multiple_of(p * features, features), features)
         total[...] += jnp.dot(scaled, held[rows, :], preferred_element_type=F32)
 
-    tp_gather(nx, slots, token_send, token_recv, consume, pause)
+    def prepare():
+        for load in small_loads:
+            load.wait()
+        reference = key_gates(mine * (size - 1) + c * z)[:, height - 1 : height]
+        for slot in range(size):
+            relative = reference - key_gates(slot)
+            for head in range(2):
+                bias[slot, head] = jnp.transpose(jnp.broadcast_to(relative[head : head + 1], (128, height)))
+        top[...] = jnp.full(top.shape, LOW, F32)
+        acc[...] = jnp.zeros_like(acc)
+
+    tp_gather(nx, slots, token_send, token_recv, consume, prepare, pause)
+    reference_gate = key_gates(mine * (size - 1) + c * z)[:, height - 1 : height]
     mean = jnp.sum(squares[...], axis=1, keepdims=True) / held.shape[0]
     inverse = lax.rsqrt(mean + EPSILON)
 
@@ -523,11 +554,12 @@
             b_copy(way, slot, step - 1).wait_recv()
             if 2 * step < size and way in b_ways(step + 1):
                 begin(b_copy(way, slot, step))
-        fold(step)
-        if step == 1:
+        if step == 2:
             row_states()
-        if step == 2:
+        if step == min(3, size // 2):
             all_states()
+        if step < size // 2:
+            fold(step)
 
     def o_copy(source, slot, target):
         return remote(obuf.at[slot], rbuf.at[source], o_send.at[slot], o_recv.at[source], on_b(target))
@@ -544,13 +576,46 @@
     sent = mine * (size - 1 - z) + c * (size - 1)
     received = mine * z + c * (size - 1)
 
-    @pl.loop(1, sent + 1)
-    def _(step):
+    half = size // 2
+    opposite = jnp.where(half <= reach, 1, 0)
+
+    def give(step):
         target = shifted(b, step)
         obuf[target] = jnp.concatenate(
             [piece.astype(BF16) for piece in rows_of(target)] + [padded_thirds(logs_of(target), 16)], axis=0
         )
         o_copy(b, target, target).start()
+
+    most = mine * (reach + 1 - opposite) + c * opposite * (size - 1)
+
+    def place_most(number):
+        bounded = jnp.where(number < half, number, number + 1)
+        iq = mine * (b + bounded) + c * shifted(b, number - (half - 1))
+        ik = mine * shifted(a, half) + c * (a - half)
+        return iq, ik
+
+    @pl.when(most > 0)
+    def _():
+        pipeline(most, place_most)
+
+    @pl.loop(1, sent + 1)
+    def _(step):
+        @pl.when(step != half)
+        def _():
+            give(step)
+
+    rest = mine * opposite * size + c * (reach + 1)
+
+    def place_rest(number):
+        return shifted(b, half), mine * shifted(a, number) + c * (a - number)
+
+    @pl.when(rest > 0)
+    def _():
+        pipeline(rest, place_rest)
+
+    @pl.when(sent >= half)
+    def _():
+        give(half)
 
     @pl.loop(1, size)
     def _(step):
@@ -640,7 +705,7 @@
     return pl.pallas_call(
         functools.partial(unpack, size, nx),
         out_shape=jax.ShapeDtypeStruct((height, out_width), BF16),
-        in_specs=[ANY, VM] + [ANY] * 6 + [VM] * 6 + [ANY] * 2,
+        in_specs=[ANY] * 16,
         out_specs=VM,
         scratch_shapes=[
             pltpu.VMEM((2 * nx, height, features), BF16),
@@ -649,6 +714,14 @@
             pltpu.VMEM((height, 128), F32),
             pltpu.VMEM((2 * nx, height, 256), BF16),
             pltpu.VMEM((2 * nx, 256, out_width), BF16),
+            pltpu.VMEM((2 * nx, 1, features), F32),
+            pltpu.VMEM((1, 128), F32),
+            pltpu.VMEM((1, height), F32),
+            pltpu.VMEM((128, 128), F32),
+            pltpu.VMEM((1, 128), F32),
+            pltpu.VMEM((2, gate_cache.shape[0]), F32),
+            pltpu.VMEM((1, 128), F32),
+            DMA((7,)),
             DMA,
             DMA((6,)),
             DMA((4 * nx,)),

time: 63.8 us -> 61.8 us (0.969)
  Pallas kernels: 62.1 us -> 60.1 us
    pallas_call x1, Pallas kernels: 62.1 us -> 60.1 us  [layer(): pl.pallas_call(functools.partial(unpack, size, nx), out_shape=jax.ShapeDt...]
where the time goes in v5:
time: 61.8 us; the launch traced here: 61.7 us
  Pallas kernels  60.1 us (97%)
  local copies, waits for them, and re-layouts  1.57 us (3%)
    pallas_call x1, Pallas kernels, layer(): pl.pallas_call(functools.partial(unpack, size, nx), out_shape=jax.ShapeDt...  60.1 us
    unnamed x1, local copies, waits for them, and re-layouts  1.57 us

profile of v5, /device:TPU:1, one launch (start us, length us, event | category | flops | bytes accessed | tf_op | source)
XLA Modules:
  0.0 61.7 jit_solution(6846158572842273676)
XLA Ops:
  0.0 60.1 %layer.1 = bf16[256,256]{1,0:T(8,128)(2,1)} custom-call(bf16[256,256]{1,0:T(8,128)(2,1)} %refs_0_.1, f32[8,1,256]{2,1,0:T(1,128)} %bitcast.9, bf16[2048,128]{1,0:T(8,128)(2,1)} %refs_2_.1, bf16[2048,128]{1,0:T(8,128)(2,1)} %refs_3_.1, bf16[2048,128]{1,0:T(8,128)(2,1)} %refs_4_.1, bf16[2048,128]{1,0:T(8,128)(2,1)} %refs_5_.1, bf16[2048,128]{1,0:T(8,128)(2,1)} %refs_6_.1, ...), custom_call_target="tpu_custom_call" | custom-call | tf_op jit(solution)/shard_map/layer/pallas_call | solution.py:705
  60.1 1.6 %copy.18 = bf16[256,256]{1,0:T(8,128)(2,1)} copy(bf16[256,256]{1,0:T(8,128)(2,1)} %layer.1) | data formatting | bytes 262144

commit v6 on v5

--- a/solution.py
+++ b/solution.py
@@ -571,7 +571,7 @@
         ]
 
     def rows_of(iq):
-        return [acc[iq, head][:FD] / acc[iq, head][FD : FD + 1] for head in range(2)]
+        return [acc[iq, head][:FD] * (1.0 / acc[iq, head][FD : FD + 1]) for head in range(2)]
 
     sent = mine * (size - 1 - z) + c * (size - 1)
     received = mine * z + c * (size - 1)
@@ -648,7 +648,7 @@
     merged = lax.fori_loop(1, received + 1, merge, tuple(start))
     normed = []
     for head in range(2):
-        rows = merged[3 * head + 2] / merged[3 * head + 1]
+        rows = merged[3 * head + 2] * (1.0 / merged[3 * head + 1])
         mean = jnp.mean(rows * rows, axis=0, keepdims=True)
         normed.append(rows * lax.rsqrt(mean + EPSILON))
     att_rows = jnp.transpose(jnp.concatenate(normed, axis=0))

time: 61.8 us -> 61.8 us (level)
  no operation moved by 1% of the time
where the time goes in v6:
time: 61.8 us; the launch traced here: 61.7 us
  Pallas kernels  60.1 us (97%)
  local copies, waits for them, and re-layouts  1.57 us (3%)
    pallas_call x1, Pallas kernels, layer(): pl.pallas_call(functools.partial(unpack, size, nx), out_shape=jax.ShapeDt...  60.1 us
    unnamed x1, local copies, waits for them, and re-layouts  1.57 us

profile of v6, /device:TPU:1, one launch (start us, length us, event | category | flops | bytes accessed | tf_op | source)
XLA Modules:
  0.0 61.7 jit_solution(1287228890692568835)
XLA Ops:
  0.0 60.1 %layer.1 = bf16[256,256]{1,0:T(8,128)(2,1)} custom-call(bf16[256,256]{1,0:T(8,128)(2,1)} %refs_0_.1, f32[8,1,256]{2,1,0:T(1,128)} %bitcast.9, bf16[2048,128]{1,0:T(8,128)(2,1)} %refs_2_.1, bf16[2048,128]{1,0:T(8,128)(2,1)} %refs_3_.1, bf16[2048,128]{1,0:T(8,128)(2,1)} %refs_4_.1, bf16[2048,128]{1,0:T(8,128)(2,1)} %refs_5_.1, bf16[2048,128]{1,0:T(8,128)(2,1)} %refs_6_.1, ...), custom_call_target="tpu_custom_call" | custom-call | tf_op jit(solution)/shard_map/layer/pallas_call | solution.py:705
  60.1 1.6 %copy.18 = bf16[256,256]{1,0:T(8,128)(2,1)} copy(bf16[256,256]{1,0:T(8,128)(2,1)} %layer.1) | data formatting | bytes 262144
